TPU v7x, 512 devices: a whole 4x4x16 slice. The times are simulated.
512 devices in a mesh: sp: 64 (over z, y), tp: 8 (over x, core).
Axes of the slice: x: 4, y: 4, z: 16, core: 2. Of those that a mesh axis runs over, the one named last changes fastest.
Arguments:
- target: bfloat16 [8192, 2048], P('sp'), may hold values from -0.375 to 0.375
- source: bfloat16 [16384, 2048], P(('sp', 'tp')), may hold values from -0.375 to 0.375
- target_gain: float32 [2048], replicated, may hold values from 0.3 to 12
- source_gain: float32 [2048], replicated, may hold values from 0.3 to 12
- w_query: bfloat16 [2048, 1024], P(None, 'tp'), may hold values from -0.125 to 0.125
- w_key: bfloat16 [2048, 256], replicated, may hold values from -0.125 to 0.125
- w_value: bfloat16 [2048, 256], replicated, may hold values from -0.125 to 0.125
- attended: bfloat16 [8192, 1024], P('sp', 'tp'), may hold values from -6 to 6
- d_attended: bfloat16 [8192, 1024], P('sp', 'tp'), may hold values from -24 to 24
Outputs:
- d_target: bfloat16 [8192, 2048], P('sp')
- d_source: float32 [16384, 2048], P(('sp', 'tp'))
- d_w_query: float32 [2048, 1024], P('sp', 'tp')
All inputs are finite; a program needn't handle non-finite values.
Results may differ from a plain program's by a relative error of at most 0.02.
The roundings to bfloat16 on the way count: a program that leaves them out, or rounds other values in their place, can miss the bound.
Values may be sent and summed in bfloat16 or wider, within the bound.
A program may use at most 64 MiB of HBM per device.

v0:
```python
import jax
import jax.numpy as jnp
from jax import lax
from jax.sharding import Mesh
from jax.sharding import PartitionSpec as P

KVH = 2
HD = 128
SP = ("sp_0", "sp_1")
SP_TP = ("sp_0", "sp_1", "tp")


EPS = 1e-06


def sent_together(arrays, axis, dim, along):
    widths = [a.shape[along] for a in arrays]
    both = jnp.concatenate(arrays, axis=along)
    result = lax.all_gather(both, axis, axis=dim, tiled=True)
    return tuple(jnp.split(result, [sum(widths[:k]) for k in range(1, len(widths))], axis=along))


def joined_all(shard, axes, combine):
    for axis in axes:
        pieces = jax.tree.map(lambda part: lax.all_gather(part, axis), shard)
        shard = jax.tree.map(lambda part: part[0], pieces)
        for k in range(1, lax.axis_size(axis)):
            shard = combine(shard, jax.tree.map(lambda part: part[k], pieces))
    return shard


def in_blocks(shard, dim, peers):
    shape = shard.shape
    pieces = shard.reshape(*shape[:dim], peers, shape[dim] // peers, *shape[dim + 1 :])
    return jnp.moveaxis(pieces, dim, 0)


def sent_and_summed(shard, axis, dim):
    pieces = in_blocks(shard, dim, lax.axis_size(axis))
    arrived = lax.all_to_all(pieces, axis, split_axis=0, concat_axis=0, tiled=True)
    return arrived.sum(axis=0)


def summed_on_arrival(shard, axis, dim):
    peers = lax.axis_size(axis)
    pieces = lax.all_to_all(in_blocks(shard, dim, peers), axis, 0, 0, tiled=True)
    return jnp.sum(pieces.astype(jnp.float32), axis=0)


def joined_along(pieces, dim):
    pieces = jnp.moveaxis(pieces, 0, dim)
    shape = pieces.shape
    return pieces.reshape(*shape[:dim], shape[dim] * shape[dim + 1], *shape[dim + 2 :])


def copy_for_each(shard, axis):
    peers = lax.axis_size(axis)
    return lax.all_to_all(
        jnp.broadcast_to(shard[None], (peers, *shard.shape)), axis, 0, 0, tiled=True
    )


def gathered_copies(shard, axis, dim):
    return joined_along(copy_for_each(shard, axis), dim)


def norm_rows(matrix, gain_vector):
    widened = matrix.astype(jnp.float32)
    inverse = lax.rsqrt(jnp.mean(widened * widened, axis=-1, keepdims=True) + EPS)
    return widened * inverse * gain_vector


def norm_back(matrix, gain_vector, cotangent):
    _, pullback = jax.vjp(lambda values: norm_rows(values, gain_vector), matrix.astype(jnp.float32))
    return pullback(cotangent)[0]


def block_count(row_count, most_rows):
    number = 1
    while row_count % (number * 2) == 0 and row_count // number > most_rows:
        number = number * 2
    return number


def merge_totals(earlier, latter):
    maxima = jnp.maximum(earlier[0], latter[0])
    totals = earlier[1] * jnp.exp(earlier[0] - maxima) + latter[1] * jnp.exp(latter[0] - maxima)
    return (maxima, totals)


def block_totals(queries, key_head, scaling):
    row_count = queries.shape[0]
    per_head = queries.reshape(row_count, -1, key_head.shape[1])
    scores = (
        jnp.einsum("rhd,sd->rhs", per_head, key_head, preferred_element_type=jnp.float32) * scaling
    )
    maxima = jnp.max(scores, axis=-1)
    totals = jnp.sum(jnp.exp(scores - maxima[..., None]), axis=-1)
    return (maxima, totals)


def score_grads(query_heads, grad_heads, delta_rows, log_total, key_head, value_head, scaling):
    scores = (
        jnp.einsum("rhd,sd->rhs", query_heads, key_head, preferred_element_type=jnp.float32)
        * scaling
    )
    weights = jnp.exp(scores - log_total[..., None])
    d_weights = jnp.einsum(
        "rhd,sd->rhs", grad_heads, value_head, preferred_element_type=jnp.float32
    )
    d_scores = (weights * (d_weights - delta_rows.astype(jnp.float32)[..., None])).astype(
        jnp.bfloat16
    )
    return (weights, d_scores)


def gradient_block(carried, blocks, key_head, value_head, scaling):
    key_acc, value_acc = carried
    queries, cotangent, delta_rows, log_total = blocks
    row_count = queries.shape[0]
    head_dim = key_head.shape[1]
    query_heads = queries.reshape(row_count, -1, head_dim)
    grad_heads = cotangent.reshape(row_count, -1, head_dim)
    weights, d_scores = score_grads(
        query_heads, grad_heads, delta_rows, log_total, key_head, value_head, scaling
    )
    key_acc = (
        key_acc
        + jnp.einsum("rhs,rhd->sd", d_scores, query_heads, preferred_element_type=jnp.float32)
        * scaling
    )
    value_acc = value_acc + jnp.einsum(
        "rhs,rhd->sd", weights.astype(jnp.bfloat16), grad_heads, preferred_element_type=jnp.float32
    )
    return ((key_acc, value_acc), None)


def local(target, source, target_gain, source_gain, w_query, w_key, w_value, attended, d_attended):
    tp_size = lax.axis_size("tp")
    local_rows = target.shape[0]
    source_rows = source.shape[0]
    query_width = w_query.shape[1]
    scaling = HD ** (-0.5)
    normed_target = norm_rows(target, target_gain).astype(jnp.bfloat16)
    normed_source = norm_rows(source, source_gain).astype(jnp.bfloat16)
    query = jnp.dot(normed_target, w_query, preferred_element_type=jnp.float32).astype(jnp.bfloat16)
    key_own = jnp.dot(normed_source, w_key, preferred_element_type=jnp.float32).astype(jnp.bfloat16)
    value_own = jnp.dot(normed_source, w_value, preferred_element_type=jnp.float32).astype(
        jnp.bfloat16
    )
    key_block, value_block = sent_together((key_own, value_own), "tp", 0, 1)
    group_size = tp_size // KVH
    kv_index = lax.axis_index("tp") // group_size
    key_head = lax.dynamic_slice_in_dim(key_block, kv_index * HD, HD, 1)
    value_head = lax.dynamic_slice_in_dim(value_block, kv_index * HD, HD, 1)
    delta = jnp.einsum(
        "rhd,rhd->rh",
        d_attended.reshape(local_rows, -1, HD),
        attended.reshape(local_rows, -1, HD),
        preferred_element_type=jnp.float32,
    ).astype(jnp.bfloat16)
    all_queries = lax.all_gather(query, SP, axis=0, tiled=True)
    target_total = all_queries.shape[0]
    number = block_count(target_total, 512)
    maxima, totals = lax.map(
        lambda blocked: block_totals(blocked, key_head, scaling),
        all_queries.reshape(number, target_total // number, query_width),
    )
    maxima = maxima.reshape(target_total, -1)
    totals = totals.reshape(target_total, -1)
    maxima, totals = joined_all((maxima, totals), SP, merge_totals)
    log_total = maxima + jnp.log(totals)
    block_rows = key_head.shape[0]
    start_state = (
        jnp.zeros((block_rows, HD), jnp.float32),
        jnp.zeros((block_rows, HD), jnp.float32),
    )
    key_acc = start_state[0]
    value_acc = start_state[1]
    cotangent, delta_piece = sent_together((d_attended, delta), SP, 0, 1)
    row_count = cotangent.shape[0]
    pieces_count = block_count(row_count, 512)
    blocked = tuple(
        (
            member.reshape((pieces_count, row_count // pieces_count) + member.shape[1:])
            for member in (all_queries, cotangent, delta_piece, log_total)
        )
    )

    def fold_inner_step(state, blocks):
        return gradient_block(state, blocks, key_head, value_head, scaling)

    (key_acc, value_acc), grad_rows = lax.scan(fold_inner_step, (key_acc, value_acc), blocked)
    folded = (key_acc, value_acc)
    key_acc = folded[0]
    value_acc = folded[1]
    own_totals = lax.dynamic_slice_in_dim(log_total, lax.axis_index(SP) * local_rows, local_rows, 0)
    own_queries = query.reshape(local_rows, -1, HD)
    own_grads = d_attended.reshape(local_rows, -1, HD)
    query_start = jnp.zeros((local_rows, query_width // HD, HD), jnp.float32)
    keys_piece, values_piece = sent_together((key_head, value_head), SP, 0, 1)
    row_count = keys_piece.shape[0]
    pieces_count = block_count(row_count, 512)
    key_blocks = keys_piece.reshape(pieces_count, row_count // pieces_count, HD)
    value_blocks = values_piece.reshape(pieces_count, row_count // pieces_count, HD)

    def key_inner_step(state, blocks):
        keys_now, values_now = blocks
        _, d_scores = score_grads(
            own_queries, own_grads, delta, own_totals, keys_now, values_now, scaling
        )
        return (
            state
            + jnp.einsum("rhs,sd->rhd", d_scores, keys_now, preferred_element_type=jnp.float32)
            * scaling,
            None,
        )

    result, _ = lax.scan(key_inner_step, query_start, (key_blocks, value_blocks))
    d_query = result.reshape(local_rows, query_width).astype(jnp.bfloat16)
    d_w_query = sent_and_summed(
        jnp.einsum("rd,rc->dc", normed_target, d_query, preferred_element_type=jnp.float32), SP, 0
    )
    share_rows = local_rows // tp_size
    grad_rows = d_query
    d_normed = summed_on_arrival(
        jnp.einsum("rc,dc->rd", grad_rows, w_query, preferred_element_type=jnp.float32).astype(
            jnp.bfloat16
        ),
        "tp",
        0,
    )
    own_rows = lax.dynamic_slice_in_dim(target, lax.axis_index("tp") * share_rows, share_rows, 0)
    own_grad = norm_back(own_rows, target_gain, d_normed).astype(jnp.bfloat16)
    d_target = gathered_copies(own_grad, "tp", 0)
    stacked = jnp.stack([key_acc, value_acc], axis=1).reshape(tp_size, source_rows, 2 * HD)
    returned = lax.all_to_all(
        stacked.astype(jnp.bfloat16), "tp", split_axis=0, concat_axis=0, tiled=True
    ).astype(stacked.dtype)
    grouped = returned.reshape(KVH, group_size, source_rows, 2, HD).sum(axis=1)
    d_key = (
        grouped[:, :, 0, :].transpose(1, 0, 2).reshape(source_rows, KVH * HD).astype(jnp.bfloat16)
    )
    d_value = (
        grouped[:, :, 1, :].transpose(1, 0, 2).reshape(source_rows, KVH * HD).astype(jnp.bfloat16)
    )
    d_normed_source = jnp.einsum(
        "rc,dc->rd", d_key, w_key, preferred_element_type=jnp.float32
    ) + jnp.einsum("rc,dc->rd", d_value, w_value, preferred_element_type=jnp.float32)
    d_source = norm_back(source, source_gain, d_normed_source)
    return (d_target, d_source, d_w_query)


def solution(mesh):
    finer = Mesh(mesh.devices.reshape(16, 4, mesh.shape["tp"]), ("sp_0", "sp_1", "tp"))
    placed = (
        P(SP, None),
        P(SP_TP, None),
        P(),
        P(),
        P(None, "tp"),
        P(),
        P(),
        P(SP, "tp"),
        P(SP, "tp"),
    )
    return jax.shard_map(
        local,
        mesh=finer,
        in_specs=placed,
        out_specs=(P(SP, None), P(SP_TP, None), P(SP, "tp")),
        check_vma=False,
    )
```

profile of v0, /device:TPU:1, one launch (start us, length us, event | category | flops | bytes accessed | tf_op | source)
XLA Modules:
  0.0 656.3 jit_solution(8378921525425368850)
XLA Ops:
  10.1 2.0 convolution_convert_fusion.1
  17.0 19.5 %all_gather.26 = bf16[256,512]{1,0:T(8,128)(2,1)S(1)} all-gather(bf16[32,512]{1,0:T(8,128)(2,1)S(1)} %pad_maximum_fusion.3), channel_id=1, replica_groups=mesh['sp_0'=16,'sp_1'=4,'tp'=8] {'tp'}, dimensions={0}, use_global_device_ids=true | all-gather | bytes 294912 | tf_op jit(solution)/shard_map/all_gather | solution.py:19
  37.3 111.4 %all-gather.6.cloned.1.call-done = bf16[8192,128]{1,0:T(8,128)(2,1)} async-done(((bf16[128,128]{1,0:T(8,128)(2,1)}), bf16[8192,128]{1,0:T(8,128)(2,1)}) %all-gather.6.cloned.1.call-update) | async-done | bytes 2097168 | tf_op jit(solution)/shard_map/all_gather | solution.py:162
  148.7 20.6 %while.36 = (s32[]{:T(128)}, f32[16,512,1]{1,2,0:T(1,128)S(1)}, f32[16,512,1]{1,2,0:T(1,128)S(1)}, bf16[16,512,128]{2,1,0:T(8,128)(2,1)}, bf16[256,128]{1,0:T(8,128)(2,1)S(1)}, /*index=5*/s32[]{:T(128)}) while((s32[]{:T(128)}, f32[16,512,1]{1,2,0:T(1,128)S(1)}, f32[16,512,1]{1,2,0:T(1,128)S(1)}, bf16[16,512,128]{2,1,0:T(8,128)(2,1)}, ...), condition=%wide.region_5.6_spmd, body=%wide.region_2.5_spmd.sunk | while | flops 34077696 | bytes 1259605 | solution.py:165
  169.3 25.1 %all_gather.31 = f32[16,8192,1]{1,2,0:T(1,128)S(1)} all-gather(f32[1,8192,1]{1,2,0:T(1,128)S(1)} %bitcast.234), channel_id=1, replica_groups=mesh['sp_0'=16,'sp_1'=4,'tp'=8] {'sp_0'}, dimensions={0}, use_global_device_ids=true | all-gather | bytes 557056 | tf_op jit(solution)/shard_map/all_gather | solution.py:25
  194.4 24.5 %all_gather.29 = f32[16,8192,1]{1,2,0:T(1,128)S(1)} all-gather(f32[1,8192,1]{1,2,0:T(1,128)} %bitcast.233), channel_id=1, replica_groups=mesh['sp_0'=16,'sp_1'=4,'tp'=8] {'sp_0'}, dimensions={0}, use_global_device_ids=true | all-gather | bytes 557056 | tf_op jit(solution)/shard_map/all_gather | solution.py:25
  220.3 9.8 %all_gather.30 = f32[4,8192,1]{1,2,0:T(1,128)S(1)} all-gather(f32[1,8192,1]{1,2,0:T(1,128)S(1)} %get-tuple-element.240), channel_id=1, replica_groups=mesh['sp_0'=16,'sp_1'=4,'tp'=8] {'sp_1'}, dimensions={0}, use_global_device_ids=true | all-gather | bytes 163840 | tf_op jit(solution)/shard_map/all_gather | solution.py:25
  230.2 9.1 %all_gather.32 = f32[4,8192,1]{1,2,0:T(1,128)S(1)} all-gather(f32[1,8192,1]{1,2,0:T(1,128)S(1)} %get-tuple-element.239), channel_id=1, replica_groups=mesh['sp_0'=16,'sp_1'=4,'tp'=8] {'sp_1'}, dimensions={0}, use_global_device_ids=true | all-gather | bytes 163840 | tf_op jit(solution)/shard_map/all_gather | solution.py:25
  240.3 54.3 %all-gather.8.cloned.1.call-done = bf16[8192,129]{1,0:T(8,128)(2,1)} async-done(((bf16[128,129]{1,0:T(8,128)(2,1)}), bf16[8192,129]{1,0:T(8,128)(2,1)}) %all-gather.8.cloned.1.call-update) | async-done | bytes 2113552 | tf_op jit(solution)/shard_map/all_gather | solution.py:19
  294.6 2.2 slice_reduce_fusion
  297.4 3.0 split.28
  300.5 84.5 %while.38 = (s32[]{:T(128)}, f32[256,128]{1,0:T(8,128)S(1)}, f32[256,128]{1,0:T(8,128)S(1)}, bf16[16,512,128]{2,1,0:T(8,128)(2,1)}, bf16[256,128]{1,0:T(8,128)(2...) while((s32[]{:T(128)}, f32[256,128]{1,0:T(8,128)S(1)}, ...), condition=%wide.region_12.13_spmd.clone, body=%wide.region_11.12_spmd.clone.sunk | while | flops 135168512 | bytes 2765455 | solution.py:193
  385.0 65.5 %all-gather.4.cloned.1.call-done = bf16[16384,256]{1,0:T(8,128)(2,1)} async-done(((bf16[256,256]{1,0:T(8,128)(2,1)}), bf16[16384,256]{1,0:T(8,128)(2,1)}) %all-gather.4.cloned.1.call-update) | async-done | bytes 8388624 | tf_op jit(solution)/shard_map/all_gather | solution.py:19
  450.5 5.7 fusion.125
  456.2 81.4 %while.37 = (s32[]{:T(128)}, f32[128,1,128]{2,0,1:T(8,128)S(1)}, bf16[32,512,128]{2,1,0:T(8,128)(2,1)}, bf16[128,1,128]{2,0,1:T(8,128)(2,1)S(1)}, f32[128,1]{0,1...) while((s32[]{:T(128)}, f32[128,1,128]{2,0,1:T(8,128)S(1)}, ...), condition=%wide.region_7.8_spmd.clone, body=%wide.region_6.7_spmd.clone.sunk | while | flops 50708608 | bytes 1117562 | solution.py:219
  537.6 2.1 convolution_convert_fusion
  539.8 12.7 %all-to-all-start = ((bf16[8,16,2048]{2,1,0:T(8,128)(2,1)}), bf16[8,16,2048]{2,1,0:T(8,128)(2,1)}, u32[]{:S(2)}, u32[]{:S(2)}) async-start(bf16[8,16,2048]{2,1,0:T(8,128)(2,1)} %bitcast.217), calls=%async_computation | async-start | bytes 1048576 | tf_op jit(solution)/shard_map/all_to_all | solution.py:46
  553.4 8.5 %all-to-all-done = bf16[8,16,2048]{2,1,0:T(8,128)(2,1)} async-done(((bf16[8,16,2048]{2,1,0:T(8,128)(2,1)}), bf16[8,16,2048]{2,1,0:T(8,128)(2,1)}, u32[]{:S(2)}, u32[]{:S(2)}) %all-to-all-start) | async-done | bytes 524320 | tf_op jit(solution)/shard_map/all_to_all | solution.py:46
  561.9 4.2 all-to-all-start.2
  569.2 2.2 all-to-all-done.2
  572.2 5.0 all-to-all-start.1
  578.5 8.2 %all-to-all-done.1 = bf16[8,16,2048]{2,1,0:T(8,128)(2,1)} async-done(((bf16[8,16,2048]{2,1,0:T(8,128)(2,1)}), bf16[8,16,2048]{2,1,0:T(8,128)(2,1)}, u32[]{:S(2)}, u32[]{:S(2)}) %all-to-all-start.1) | async-done | bytes 524320 | tf_op jit(solution)/shard_map/all_to_all | solution.py:58
  586.8 8.9 %all-to-all-start.3 = ((f32[64,32,128]{2,1,0:T(8,128)}), f32[64,32,128]{2,1,0:T(8,128)S(1)}, u32[]{:S(2)}, u32[]{:S(2)}) async-start(f32[64,32,128]{2,1,0:T(8,128)} %fusion.92), calls=%async_computation.3 | async-start | bytes 2097152 | tf_op jit(solution)/shard_map/all_to_all | solution.py:40
  598.7 48.5 %all-to-all-done.3 = f32[64,32,128]{2,1,0:T(8,128)S(1)} async-done(((f32[64,32,128]{2,1,0:T(8,128)}), f32[64,32,128]{2,1,0:T(8,128)S(1)}, u32[]{:S(2)}, u32[]{:S(2)}) %all-to-all-start.3) | async-done | bytes 1048608 | tf_op jit(solution)/shard_map/all_to_all | solution.py:40
  (313 shorter events, 207.4 us)
Async XLA Ops:
  7.2 9.1 %copy-start = (bf16[2048,256]{1,0:T(8,128)(2,1)S(1)}, bf16[2048,256]{1,0:T(8,128)(2,1)}, u32[]{:S(2)}) copy-start(bf16[2048,256]{1,0:T(8,128)(2,1)} %param.21) | copy-start | bytes 3145732
  7.2 9.1 %copy-start.2 = (bf16[32,2048]{1,0:T(8,128)(2,1)S(1)}, bf16[32,2048]{1,0:T(8,128)(2,1)}, u32[]{:S(2)}) copy-start(bf16[32,2048]{1,0:T(8,128)(2,1)} %param.16) | copy-start | bytes 393220
  7.2 9.1 %copy-start.8 = (f32[2048]{0:T(1024)S(1)}, f32[2048]{0:T(1024)}, u32[]{:S(2)}) copy-start(f32[2048]{0:T(1024)} %param.18) | copy-start | bytes 24580
  7.2 9.4 %copy-start.1 = (bf16[2048,256]{1,0:T(8,128)(2,1)S(1)}, bf16[2048,256]{1,0:T(8,128)(2,1)}, u32[]{:S(2)}) copy-start(bf16[2048,256]{1,0:T(8,128)(2,1)} %param.20) | copy-start | bytes 3145732
  7.2 141.5 %all-gather.6.cloned.1.call-start = ((), (), s32[]{:S(2)}) async-start(), calls=%async_computation.5 | async-start | bytes 2129920 | tf_op jit(solution)/shard_map/all_gather | solution.py:162
  12.1 282.5 %all-gather.8.cloned.1.call-start = ((), (), s32[]{:S(2)}) async-start(), calls=%async_computation.6 | async-start | bytes 4259840 | tf_op jit(solution)/shard_map/all_gather | solution.py:19
  13.0 2.7 copy-start.13
  14.6 435.9 %all-gather.4.cloned.1.call-start = ((), (), s32[]{:S(2)}) async-start(), calls=%async_computation.4 | async-start | bytes 8519680 | tf_op jit(solution)/shard_map/all_gather | solution.py:19
  15.7 0.6 copy-start.15
  16.3 20.2 %copy-start.11 = (f32[32]{0:T(128)}, f32[32]{0:T(128)S(1)}, u32[]{:S(2)}) copy-start(f32[32]{0:T(128)S(1)} %fusion.122) | copy-start | bytes 388
  169.3 25.1 %copy-start.10 = (f32[16,512,1]{1,2,0:T(1,128)}, f32[16,512,1]{1,2,0:T(1,128)S(1)}, u32[]{:S(2)}) copy-start(f32[16,512,1]{1,2,0:T(1,128)S(1)} %get-tuple-element.121) | copy-start | bytes 98308
  384.9 71.3 %copy-start.4 = (f32[128,1,128]{2,0,1:T(8,128)S(1)}, f32[128,1,128]{2,0,1:T(8,128)}, u32[]{:S(2)}) copy-start(f32[128,1,128]{2,0,1:T(8,128)} %custom-call) | copy-start | bytes 196612
  384.9 71.2 %copy-start.5 = (bf16[128,128]{1,0:T(8,128)(2,1)S(1)}, bf16[128,128]{1,0:T(8,128)(2,1)}, u32[]{:S(2)}) copy-start(bf16[128,128]{1,0:T(8,128)(2,1)} %convolution_convert_fusion.1) | copy-start | bytes 98308
  385.0 71.2 %copy-start.6 = (bf16[128,128]{1,0:T(8,128)(2,1)S(1)}, bf16[128,128]{1,0:T(8,128)(2,1)}, u32[]{:S(2)}) copy-start(bf16[128,128]{1,0:T(8,128)(2,1)} %param.23) | copy-start | bytes 98308
  385.0 71.2 %copy-start.14 = (bf16[128]{0:T(256)(128)(2,1)S(1)}, bf16[128]{0:T(256)(128)(2,1)}, u32[]{:S(2)}) copy-start(bf16[128]{0:T(256)(128)(2,1)} %copy-done.13) | copy-start | bytes 772
  456.2 111.1 %copy-start.9 = (f32[2048]{0:T(1024)S(1)}, f32[2048]{0:T(1024)}, u32[]{:S(2)}) copy-start(f32[2048]{0:T(1024)} %param.17) | copy-start | bytes 24580
  539.8 22.1 %all-to-all-start = ((bf16[8,16,2048]{2,1,0:T(8,128)(2,1)}), bf16[8,16,2048]{2,1,0:T(8,128)(2,1)}, u32[]{:S(2)}, u32[]{:S(2)}) async-start(bf16[8,16,2048]{2,1,0:T(8,128)(2,1)} %bitcast.217), calls=%async_computation | async-start | bytes 1048576 | tf_op jit(solution)/shard_map/all_to_all | solution.py:46
  561.9 9.5 %all-to-all-start.2 = ((bf16[8,32,256]{2,1,0:T(8,128)(2,1)}), bf16[8,32,256]{2,1,0:T(8,128)(2,1)S(1)}, u32[]{:S(2)}, u32[]{:S(2)}) async-start(bf16[8,32,256]{2,1,0:T(8,128)(2,1)} %convert_element_type.121), calls=%async_computation.2 | async-start | bytes 262144 | tf_op jit(solution)/shard_map/all_to_all | solution.py:237
  566.1 31.1 %copy-start.3 = (bf16[32,2048]{1,0:T(8,128)(2,1)S(1)}, bf16[32,2048]{1,0:T(8,128)(2,1)}, u32[]{:S(2)}) copy-start(bf16[32,2048]{1,0:T(8,128)(2,1)} %param.16) | copy-start | bytes 393220
  571.4 15.4 %copy-start.7 = (bf16[8,32,256]{2,1,0:T(8,128)(2,1)}, bf16[8,32,256]{2,1,0:T(8,128)(2,1)S(1)}, u32[]{:S(2)}) copy-start(bf16[8,32,256]{2,1,0:T(8,128)(2,1)S(1)} %all-to-all-done.2) | copy-start | bytes 393220
  572.2 25.6 %copy-start.16 = (f32[32]{0:T(128)S(1)}, f32[32]{0:T(128)}, u32[]{:S(2)}) copy-start(f32[32]{0:T(128)} %copy-done.15) | copy-start | bytes 388
  572.2 25.6 %copy-start.12 = (f32[32]{0:T(128)S(1)}, f32[32]{0:T(128)}, u32[]{:S(2)}) copy-start(f32[32]{0:T(128)} %copy-done.11) | copy-start | bytes 388
  572.2 14.5 %all-to-all-start.1 = ((bf16[8,16,2048]{2,1,0:T(8,128)(2,1)}), bf16[8,16,2048]{2,1,0:T(8,128)(2,1)}, u32[]{:S(2)}, u32[]{:S(2)}) async-start(bf16[8,16,2048]{2,1,0:T(8,128)(2,1)} %broadcast_in_dim.22), calls=%async_computation.1 | async-start | bytes 1048576 | tf_op jit(solution)/shard_map/all_to_all | solution.py:58
  586.8 60.4 %all-to-all-start.3 = ((f32[64,32,128]{2,1,0:T(8,128)}), f32[64,32,128]{2,1,0:T(8,128)S(1)}, u32[]{:S(2)}, u32[]{:S(2)}) async-start(f32[64,32,128]{2,1,0:T(8,128)} %fusion.92), calls=%async_computation.3 | async-start | bytes 2097152 | tf_op jit(solution)/shard_map/all_to_all | solution.py:40
Sparse Core Ops, SparseCore 0:
  12.2 136.4 all-gather.5
  151.6 142.8 all-gather.7
  298.1 152.3 all-gather.3
where the time goes:
time: 664 us; the launch traced here: 656 us
  waiting for transfers between devices  299 us (45%)
  matrix products  167 us (25%)
  blocking collectives  88 us (13%)
  starting transfers between devices  31 us (5%)
  local copies, waits for them, and re-layouts  29.6 us (4%)
  other arithmetic  25.7 us (4%)
  between operations  14.2 us (2%)
    all_gather x2, waiting for transfers between devices, sent_together(): result = lax.all_gather(both, axis, axis=dim, tiled=True)  120 us
    all_gather x1, waiting for transfers between devices, local(): all_queries = lax.all_gather(query, SP, axis=0, tiled=True)  111 us
    all_gather x4, blocking collectives, joined_all(): pieces = jax.tree.map(lambda part: lax.all_gather(part, axis), shard)  68.5 us
    dot_general x48, matrix products, score_grads(): jnp.einsum('rhd,sd->rhs', query_heads, key_head, preferred_element_type=j...  53.7 us
    all_to_all x1, waiting for transfers between devices, sent_and_summed(): lax.all_to_all(pieces, axis, split_axis=0, concat_axis=0, tiled=True)  48.5 us
    dot_general x32, matrix products, key_inner_step(): jnp.einsum('rhs,sd->rhd', d_scores, keys_now, preferred_element_type=jnp....  44.5 us
    dot_general x16, matrix products, gradient_block(): jnp.einsum('rhs,rhd->sd', d_scores, query_heads, preferred_element_type=j...  24.2 us
    all_gather x1, blocking collectives, sent_together(): result = lax.all_gather(both, axis, axis=dim, tiled=True)  19.5 us
  transfers between devices with their start and end apart: 7, of which 7 were waited for; matrix products, arithmetic and copies ran while one was open for 19% of the time, Pallas kernels for 0%

commit v1 on v0

v1 whole, which is shorter than its diff:
```python
import functools
import math

import jax
import jax.numpy as jnp
from jax import lax
from jax.experimental import pallas as pl
from jax.experimental.pallas import tpu as pltpu
from jax.sharding import Mesh
from jax.sharding import PartitionSpec as P

HD = 128
EPS = 1e-06
SCALE = HD ** (-0.5)
NZ, NY, NX, NC = 16, 4, 4, 2
PLANE = 16
MESH = pl.DeviceIdType.MESH
F32 = jnp.float32
BF16 = jnp.bfloat16
NT = (((1,), (1,)), ((), ()))


def norm_rows(matrix, gain_vector):
    widened = matrix.astype(F32)
    inverse = lax.rsqrt(jnp.mean(widened * widened, axis=-1, keepdims=True) + EPS)
    return widened * inverse * gain_vector


def norm_back(matrix, gain_vector, cotangent):
    _, pullback = jax.vjp(lambda values: norm_rows(values, gain_vector), matrix.astype(F32))
    return pullback(cotangent)[0]


def coords():
    return tuple(lax.axis_index(a) for a in ("z", "y", "x", "c"))


def plane_peers(me, with_self=False):
    z, y, x, c = me
    out = []
    for dy in (2, 1, 3, 0):
        for dx in (1, 0):
            for dc in (1, 0):
                if (dy, dx, dc) == (0, 0, 0) and not with_self:
                    continue
                y2 = lax.rem(y + dy, NY)
                xl2 = lax.rem(lax.rem(x, 2) + dx, 2)
                c2 = lax.rem(c + dc, 2)
                out.append(((z, y2, (x // 2) * 2 + xl2, c2), y2 * 4 + xl2 * 2 + c2))
    return out


def line_peers(me):
    z, y, x, c = me
    out = []
    for dz in (8, 7, 9, 6, 10, 5, 11, 4, 12, 3, 13, 2, 14, 1, 15, 0):
        for dh in (1, 0):
            if (dz, dh) == (0, 0):
                continue
            z2 = lax.rem(z + dz, NZ)
            h2 = lax.rem(x // 2 + dh, 2)
            out.append(((z2, y, h2 * 2 + lax.rem(x, 2), c), z2, h2))
    return out


def y_peers(me):
    z, y, x, c = me
    return [((z, lax.rem(y + dy, NY), x, c), lax.rem(y + dy, NY)) for dy in (2, 1, 3)]


def z_peers(me):
    z, y, x, c = me
    order = (8, 7, 9, 6, 10, 5, 11, 4, 12, 3, 13, 2, 14, 1, 15)
    return [((lax.rem(z + dz, NZ), y, x, c), lax.rem(z + dz, NZ)) for dz in order]


def tp_peers(me):
    z, y, x, c = me
    out = []
    for dx in (2, 1, 3, 0):
        for dc in (1, 0):
            if (dx, dc) == (0, 0):
                continue
            x2 = lax.rem(x + dx, NX)
            c2 = lax.rem(c + dc, 2)
            out.append(((z, y, x2, c2), x2 * 2 + c2))
    return out


def greet(devices):
    barrier = pltpu.get_barrier_semaphore()
    for d in devices:
        pl.semaphore_signal(barrier, inc=1, device_id=d, device_id_type=MESH)
    pl.semaphore_wait(barrier, len(devices))


def exchange(copies, send, recv):
    started = []
    for k, (src, dst, dev) in enumerate(copies):
        cp = pltpu.make_async_remote_copy(
            src_ref=src, dst_ref=dst, send_sem=send.at[k], recv_sem=recv.at[k],
            device_id=dev, device_id_type=MESH)
        cp.start()
        started.append(cp)
    return started


def comm_call(body, outs, count, cid, *args):
    vm = pl.BlockSpec(memory_space=pltpu.VMEM)
    return pl.pallas_call(
        body,
        out_shape=outs,
        in_specs=[vm] * len(args),
        out_specs=[vm] * len(outs),
        scratch_shapes=[pltpu.SemaphoreType.DMA((count,)), pltpu.SemaphoreType.DMA((count,))],
        compiler_params=pltpu.CompilerParams(collective_id=cid, has_side_effects=True),
        name="comm%d" % cid,
    )(*args)


def gather_body(q, do, dl, kv, q_all, do_all, dl_all, kv_all, send, recv):
    me = coords()
    z, y, x, c = me
    plane = plane_peers(me)
    line = line_peers(me)
    mine = y * 4 + lax.rem(x, 2) * 2 + c
    rows = pl.ds(pl.multiple_of(mine * 128, 128), 128)
    xh = x // 2
    kvrows = pl.ds(pl.multiple_of(z * 64 + xh * 32, 32), 32)
    greet([d for d, _ in plane] + [d for d, _, _ in line])
    copies = [(kv.at[h2], kv_all.at[kvrows, :], d) for d, _, h2 in line]
    copies += [(q, q_all.at[rows, :], d) for d, _ in plane]
    copies += [(do, do_all.at[rows, :], d) for d, _ in plane]
    copies += [(dl, dl_all.at[mine], d) for d, _ in plane]
    started = exchange(copies, send, recv)
    q_all[rows, :] = q[...]
    do_all[rows, :] = do[...]
    dl_all[mine] = dl[...]
    kv_all[kvrows, :] = kv[xh]
    for cp in started:
        cp.wait()


def stats_body(st, st_all, send, recv):
    me = coords()
    z, y, x, c = me
    plane = plane_peers(me)
    mine = y * 4 + lax.rem(x, 2) * 2 + c
    greet([d for d, _ in plane])
    started = exchange([(st, st_all.at[mine], d) for d, _ in plane], send, recv)
    st_all[mine] = st[...]
    for cp in started:
        cp.wait()


def scatter_body(dq, dkv, dq_in, dkv_in, send, recv):
    me = coords()
    z, y, x, c = me
    plane = plane_peers(me)
    line = line_peers(me)
    mine = y * 4 + lax.rem(x, 2) * 2 + c
    xh = x // 2
    greet([d for d, _ in plane] + [d for d, _, _ in line])
    copies = [(dkv.at[z2, h2], dkv_in.at[xh, z], d) for d, z2, h2 in line]
    copies += [(dq.at[j], dq_in.at[mine], d) for d, j in plane]
    started = exchange(copies, send, recv)
    dq_in[mine] = dq[mine]
    dkv_in[xh, z] = dkv[z, xh]
    for cp in started:
        cp.wait()


def tail1_body(dw, dn, dw_in, dn_in, send, recv):
    me = coords()
    z, y, x, c = me
    ys = y_peers(me)
    tps = tp_peers(me)
    tp = x * 2 + c
    greet([d for d, _ in ys] + [d for d, _ in tps])
    copies = [(dw.at[y2], dw_in.at[y], d) for d, y2 in ys]
    copies += [(dn.at[t2], dn_in.at[tp], d) for d, t2 in tps]
    started = exchange(copies, send, recv)
    dw_in[y] = dw[y]
    dn_in[tp] = dn[tp]
    for cp in started:
        cp.wait()


def tail2_body(dw, dt, dw_in, dt_in, send, recv):
    me = coords()
    z, y, x, c = me
    zs = z_peers(me)
    tps = tp_peers(me)
    tp = x * 2 + c
    greet([d for d, _ in zs] + [d for d, _ in tps])
    copies = [(dw.at[z2], dw_in.at[z], d) for d, z2 in zs]
    copies += [(dt, dt_in.at[tp], d) for d, t2 in tps]
    started = exchange(copies, send, recv)
    dw_in[z] = dw[z]
    dt_in[tp] = dt[...]
    for cp in started:
        cp.wait()


def stats_kernel(q_all, kv_all, st, s_scr):
    def pair(p, carry):
        q = q_all[pl.ds(pl.multiple_of(p * 256, 256), 256), :]
        top = None
        for k in range(4):
            s = lax.dot_general(kv_all[k * 256:(k + 1) * 256, :128], q, NT,
                                preferred_element_type=F32) * SCALE
            s_scr[k * 256:(k + 1) * 256, :] = s
            part = jnp.max(s.reshape(32, 8, 256), axis=0)
            top = part if top is None else jnp.maximum(top, part)
        m = jnp.max(top, axis=0, keepdims=True)
        tot = None
        for k in range(4):
            e = jnp.exp(s_scr[k * 256:(k + 1) * 256, :] - m)
            part = jnp.sum(e.reshape(32, 8, 256), axis=0)
            tot = part if tot is None else tot + part
        l = jnp.sum(tot, axis=0, keepdims=True)
        st[pl.ds(2 * p, 1), :] = m[:, :128]
        st[pl.ds(2 * p + 1, 1), :] = m[:, 128:]
        st[pl.ds(2 * p + 16, 1), :] = l[:, :128]
        st[pl.ds(2 * p + 17, 1), :] = l[:, 128:]
        return carry

    lax.fori_loop(0, 8, pair, 0)


def grads_kernel(q_all, do_all, dl_all, kv_all, st_all, dq, dkv, pt, ut, kt, lt):
    kt[...] = jnp.transpose(kv_all[:, :128])
    top = jnp.max(st_all[:, 0:16, :], axis=0)
    total = jnp.zeros((16, 128), F32)
    for j in range(16):
        total = total + st_all[j, 16:32, :] * jnp.exp(st_all[j, 0:16, :] - top)
    lt[...] = top + jnp.log(total)

    def pair(p, carry):
        rows = pl.ds(pl.multiple_of(p * 256, 256), 256)
        q = q_all[rows, :]
        do = do_all[rows, :]
        lrow = jnp.concatenate([lt[pl.ds(2 * p, 1), :], lt[pl.ds(2 * p + 1, 1), :]], axis=1)
        drow = jnp.concatenate([dl_all[2 * p, 0:1, :], dl_all[2 * p + 1, 0:1, :]], axis=1)
        for k in range(4):
            blk = slice(k * 256, (k + 1) * 256)
            s = lax.dot_general(kv_all[blk, :128], q, NT, preferred_element_type=F32) * SCALE
            w = jnp.exp(s - lrow)
            pt[blk, rows] = w.astype(BF16)
            g = lax.dot_general(kv_all[blk, 128:], do, NT, preferred_element_type=F32)
            ut[blk, rows] = (w * (g - drow)).astype(BF16)
        dqt = lax.dot_general(kt[...], ut[:, rows], (((1,), (0,)), ((), ())),
                              preferred_element_type=F32) * SCALE
        dq[rows, :] = jnp.transpose(dqt).astype(BF16)
        return carry

    lax.fori_loop(0, 8, pair, 0)

    def block(k, carry):
        rows = pl.ds(pl.multiple_of(k * 256, 256), 256)
        dk = jnp.dot(ut[rows, :], q_all[...], preferred_element_type=F32) * SCALE
        dv = jnp.dot(pt[rows, :], do_all[...], preferred_element_type=F32)
        dkv[rows, :] = jnp.concatenate([dk, dv], axis=1).astype(BF16)
        return carry

    lax.fori_loop(0, 4, block, 0)


def local_call(body, outs, scratch, name, flops, *args):
    vm = pl.BlockSpec(memory_space=pltpu.VMEM)
    return pl.pallas_call(
        body,
        out_shape=outs,
        in_specs=[vm] * len(args),
        out_specs=[vm] * len(outs),
        scratch_shapes=scratch,
        compiler_params=pltpu.CompilerParams(vmem_limit_bytes=48 * 1024 * 1024),
        cost_estimate=pl.CostEstimate(flops=flops, bytes_accessed=1 << 20, transcendentals=0),
        name=name,
    )(*args)


def shape(*dims, dtype=BF16):
    return jax.ShapeDtypeStruct(dims, dtype)


def local(target, source, target_gain, source_gain, w_query, w_key, w_value, attended, d_attended):
    z, y, x, c = coords()
    nt = norm_rows(target, target_gain).astype(BF16)
    ns = norm_rows(source, source_gain).astype(BF16)
    query = jnp.dot(nt, w_query, preferred_element_type=F32).astype(BF16)
    key = jnp.dot(ns, w_key, preferred_element_type=F32).astype(BF16)
    value = jnp.dot(ns, w_value, preferred_element_type=F32).astype(BF16)
    kv = jnp.stack([jnp.concatenate([key[:, :128], value[:, :128]], axis=1),
                    jnp.concatenate([key[:, 128:], value[:, 128:]], axis=1)])
    delta = jnp.sum(d_attended.astype(F32) * attended.astype(F32), axis=-1)
    delta = lax.reduce_precision(delta, 8, 7)
    dl = jnp.broadcast_to(delta[None, :], (8, 128))

    q_all, do_all, dl_all, kv_all = comm_call(
        gather_body,
        [shape(2048, 128), shape(2048, 128), shape(16, 8, 128, dtype=F32), shape(1024, 256)],
        31 + 45, 0, query, d_attended, dl, kv)
    st, = local_call(stats_kernel, [shape(32, 128, dtype=F32)],
                     [pltpu.VMEM((1024, 256), F32)], "stats", 1 << 30, q_all, kv_all)
    st_all, = comm_call(stats_body, [shape(16, 32, 128, dtype=F32)], 15, 1, st)
    dq, dkv = local_call(
        grads_kernel, [shape(2048, 128), shape(1024, 256)],
        [pltpu.VMEM((1024, 2048), BF16), pltpu.VMEM((1024, 2048), BF16),
         pltpu.VMEM((128, 1024), BF16), pltpu.VMEM((16, 128), F32)],
        "grads", 1 << 32, q_all, do_all, dl_all, kv_all, st_all)
    dq_in, dkv_in = comm_call(
        scatter_body, [shape(16, 128, 128), shape(2, 16, 32, 256)], 46, 2,
        dq.reshape(16, 128, 128), dkv.reshape(16, 2, 32, 256))
    dqb = jnp.sum(dq_in.astype(F32), axis=0).astype(BF16)
    dw = lax.dot_general(nt, dqb, (((0,), (0,)), ((), ())), preferred_element_type=F32)
    dw = dw.astype(BF16).reshape(16, 4, 32, 128).transpose(1, 0, 2, 3)
    dn = lax.dot_general(dqb, w_query, NT, preferred_element_type=F32).astype(BF16)
    dw_in, dn_in = comm_call(tail1_body, [shape(4, 16, 32, 128), shape(8, 16, 2048)], 10, 3,
                             dw, dn.reshape(8, 16, 2048))
    dw1 = jnp.sum(dw_in.astype(F32), axis=0).astype(BF16)
    dnt = jnp.sum(dn_in.astype(F32), axis=0)
    own = lax.dynamic_slice_in_dim(target, (x * 2 + c) * 16, 16, 0)
    dt = norm_back(own, target_gain, dnt).astype(BF16)
    dw2, d_target = comm_call(tail2_body, [shape(16, 32, 128), shape(8, 16, 2048)], 22, 4, dw1, dt)
    d_w_query = jnp.sum(dw2.astype(F32), axis=0)
    dkv_sum = jnp.sum(dkv_in.astype(F32), axis=1).astype(BF16)
    dkey = jnp.concatenate([dkv_sum[0, :, :128], dkv_sum[1, :, :128]], axis=1)
    dval = jnp.concatenate([dkv_sum[0, :, 128:], dkv_sum[1, :, 128:]], axis=1)
    dns = lax.dot_general(dkey, w_key, NT, preferred_element_type=F32) + lax.dot_general(
        dval, w_value, NT, preferred_element_type=F32)
    d_source = norm_back(source, source_gain, dns)
    return d_target.reshape(128, 2048), d_source, d_w_query


def solution(mesh):
    fine = Mesh(mesh.devices.reshape(NZ, NY, NX, NC), ("z", "y", "x", "c"))
    sp = ("z", "y")
    tp = ("x", "c")
    both = ("z", "y", "x", "c")
    placed = (P(sp, None), P(both, None), P(), P(), P(None, tp), P(), P(), P(sp, tp), P(sp, tp))
    return jax.shard_map(
        local, mesh=fine, in_specs=placed,
        out_specs=(P(sp, None), P(both, None), P(sp, tp)), check_vma=False)
```

time: 664 us -> 162 us (0.24)
  waiting for transfers between devices: 299 us -> 0 us
  matrix products: 167 us -> 5.31 us
  Pallas kernels: 0 us -> 136 us
  blocking collectives: 88 us -> 0 us
  starting transfers between devices: 31 us -> 0 us
  local copies, waits for them, and re-layouts: 29.6 us -> 10.5 us
  other arithmetic: 25.7 us -> 8.47 us
  between operations: 14.2 us -> 0.92 us
    all_gather x3 -> x0, waiting for transfers between devices: 231 us -> none  [the longest x2 120 us: sent_together(): result = lax.all_gather(both, axis, axis=dim, tiled=True)]
    dot_general x135 -> x7, matrix products: 167 us -> 5.31 us  [the longest x1 1.57 us: local(): key = jnp.dot(ns, w_key, preferred_element_type=F32).astype(BF16)]
    pallas_call x0 -> x7, Pallas kernels: none -> 136 us  [the longest x5 123 us: comm_call(): pl.pallas_call(body, out_shape=outs, in_specs=[vm] * len(args), out_specs...]
    all_gather x5 -> x0, blocking collectives: 88 us -> none  [the longest x4 68.5 us: joined_all(): pieces = jax.tree.map(lambda part: lax.all_gather(part, axis), shard)]
    all_to_all x4 -> x0, waiting for transfers between devices: 67.4 us -> none  [the longest x1 48.5 us: sent_and_summed(): lax.all_to_all(pieces, axis, split_axis=0, concat_axis=0, tiled=True)]
    all_to_all x4 -> x0, starting transfers between devices: 30.9 us -> none  [the longest x1 12.7 us: summed_on_arrival(): lax.all_to_all(in_blocks(shard, dim, peers), axis, 0, 0, tiled=True)]
    convert_element_type x50 -> x1, other arithmetic: 13.4 us -> 0.73 us  [local(): dt = norm_back(own, target_gain, dnt).astype(BF16)]
    split x4 -> x0, local copies, waits for them, and re-layouts: 11 us -> none  [sent_together(): jnp.split(result, [sum(widths[:k]) for k in range(1, len(widths))], axis=...]
  transfers between devices with their start and end apart: 7 -> 0, of which waited for: 7 -> 0; matrix products, arithmetic and copies ran while one was open for 19% -> 0% of each run, Pallas kernels for 0% -> 0%
where the time goes in v1:
time: 162 us; the launch traced here: 161 us
  Pallas kernels  136 us (84%)
  local copies, waits for them, and re-layouts  10.5 us (6%)
  other arithmetic  8.47 us (5%)
  matrix products  5.31 us (3%)
    pallas_call x5, Pallas kernels, comm_call(): pl.pallas_call(body, out_shape=outs, in_specs=[vm] * len(args), out_specs...  123 us
    pallas_call x2, Pallas kernels, local_call(): pl.pallas_call(body, out_shape=outs, in_specs=[vm] * len(args), out_specs...  12.9 us
    unnamed x45, local copies, waits for them, and re-layouts  9.01 us

profile of v1, /device:TPU:1, one launch (start us, length us, event | category | flops | bytes accessed | tf_op | source)
XLA Modules:
  0.0 160.9 jit_solution(12142750677133466026)
XLA Ops:
  0.7 1.1 fusion.4
  1.8 1.6 convolution_convert_fusion.4
  5.9 1.0 convolution_convert_fusion.2.q
  7.6 44.9 %comm0.1 = (bf16[2048,128]{1,0:T(8,128)(2,1)}, bf16[2048,128]{1,0:T(8,128)(2,1)}, f32[16,8,128]{2,1,0:T(8,128)}, bf16[1024,256]{1,0:T(8,128)(2,1)}) custom-call(bf16[128,128]{1,0:T(8,128)(2,1)} %convolution_convert_fusion.2.q, bf16[128,128]{1,0:T(8,128)(2,1)} %do.1, f32[8,128]{1,0:T(8,128)} %broadcast_in_dim.6.dl, bf16[2,32,256]{2,1,0:T(8,128)(2,1)} %pad_maximum_fusion.kv), custom_call_target="tpu_custom_call" | custom-call | tf_op jit(solution)/shard_map/comm0/pallas_call | solution.py:110
  52.5 1.0 copy-done.5
  53.5 1.0 copy-done.8
  54.6 4.0 %stats.1.st = f32[32,128]{1,0:T(8,128)S(1)} custom-call(bf16[2048,128]{1,0:T(8,128)(2,1)S(1)} %copy-done.5, bf16[1024,256]{1,0:T(8,128)(2,1)S(1)} %copy-done.8), custom_call_target="tpu_custom_call" | custom-call | flops 1073741824 | bytes 1048576 | tf_op jit(solution)/shard_map/stats/pallas_call | solution.py:271
  59.2 11.9 %comm1.1.st_all = f32[16,32,128]{2,1,0:T(8,128)} custom-call(f32[32,128]{1,0:T(8,128)} %copy-done.4), custom_call_target="tpu_custom_call" | custom-call | tf_op jit(solution)/shard_map/comm1/pallas_call | solution.py:110
  71.1 0.9 copy-done.3
  72.1 8.8 %grads.1 = (bf16[2048,128]{1,0:T(8,128)(2,1)S(1)}, bf16[1024,256]{1,0:T(8,128)(2,1)S(1)}) custom-call(bf16[2048,128]{1,0:T(8,128)(2,1)S(1)} %copy-done.6, bf16[2048,128]{1,0:T(8,128)(2,1)S(1)} %copy-done.7, f32[16,8,128]{2,1,0:T(8,128)S(1)} %copy-done.10, bf16[1024,256]{1,0:T(8,128)(2,1)S(1)} %copy-done.9, f32[16,32,128]{2,1,0:T(8,128)S(1)} %copy-done.3), custom_call_target="tpu_custom_call" | custom-call | flops 4294967296 | bytes 1048576 | tf_op jit(solution)/shard_map/grads/pallas_call | solution.py:271
  80.9 0.8 copy-done.1
  81.7 0.8 copy-done.2
  82.5 35.0 %comm2.1 = (bf16[16,128,128]{2,1,0:T(8,128)(2,1)}, bf16[2,16,32,256]{3,2,1,0:T(8,128)(2,1)}) custom-call(bf16[16,128,128]{2,1,0:T(8,128)(2,1)} %bitcast.28, bf16[16,2,32,256]{3,2,1,0:T(8,128)(2,1)} %bitcast.29), custom_call_target="tpu_custom_call" | custom-call | tf_op jit(solution)/shard_map/comm2/pallas_call | solution.py:110
  117.5 1.1 reduce_sum.128
  119.6 0.8 add_add_fusion
  121.1 0.8 copy.14
  122.4 1.1 convolution_convert_fusion
  123.5 14.8 %comm3.1 = (bf16[4,16,32,128]{3,2,1,0:T(8,128)(2,1)}, bf16[8,16,2048]{2,1,0:T(8,128)(2,1)}) custom-call(bf16[4,16,32,128]{3,2,1,0:T(8,128)(2,1)} %bitcast.30, bf16[8,16,2048]{2,1,0:T(8,128)(2,1)} %bitcast.31), custom_call_target="tpu_custom_call" | custom-call | tf_op jit(solution)/shard_map/comm3/pallas_call | solution.py:110
  138.3 1.2 convert_reduce_fusion
  139.7 0.7 fusion.12.dt
  140.4 0.7 reduce_sum.124.dw
  141.1 16.3 %comm4.1 = (bf16[16,32,128]{2,1,0:T(8,128)(2,1)}, bf16[8,16,2048]{2,1,0:T(8,128)(2,1)}) custom-call(bf16[16,32,128]{2,1,0:T(8,128)(2,1)} %reduce_sum.124.dw, bf16[16,2048]{1,0:T(8,128)(2,1)} %fusion.12.dt), custom_call_target="tpu_custom_call" | custom-call | tf_op jit(solution)/shard_map/comm4/pallas_call | solution.py:110
  157.5 1.5 convert_reduce_fusion.1
  159.0 1.9 %copy.16 = bf16[128,2048]{1,0:T(8,128)(2,1)} copy(bf16[128,2048]{1,0:T(8,128)(2,1)} %bitcast.33) | data formatting | bytes 1048576
  (58 shorter events, 6.0 us)
Async XLA Ops:
  0.6 2.8 %copy-start = (bf16[2048,256]{1,0:T(8,128)(2,1)S(1)}, bf16[2048,256]{1,0:T(8,128)(2,1)}, u32[]{:S(2)}) copy-start(bf16[2048,256]{1,0:T(8,128)(2,1)} %param.15) | copy-start | bytes 3145732
  0.6 1.2 copy-start.12
  3.4 0.7 copy-start.19
  4.1 1.0 copy-start.13
  4.4 1.1 copy-start.15
  5.1 0.7 copy-start.20
  5.9 1.0 copy-start.18
  5.9 1.0 copy-start.21
  52.5 1.0 copy-start.5
  53.5 1.0 copy-start.8
  54.6 16.5 %copy-start.6 = (bf16[2048,128]{1,0:T(8,128)(2,1)S(1)}, bf16[2048,128]{1,0:T(8,128)(2,1)}, u32[]{:S(2)}) copy-start(bf16[2048,128]{1,0:T(8,128)(2,1)} %get-tuple-element.15.q_all) | copy-start | bytes 1572868
  54.6 16.6 %copy-start.7 = (bf16[2048,128]{1,0:T(8,128)(2,1)S(1)}, bf16[2048,128]{1,0:T(8,128)(2,1)}, u32[]{:S(2)}) copy-start(bf16[2048,128]{1,0:T(8,128)(2,1)} %get-tuple-element.16.do_all) | copy-start | bytes 1572868
  54.6 16.6 %copy-start.9 = (bf16[1024,256]{1,0:T(8,128)(2,1)S(1)}, bf16[1024,256]{1,0:T(8,128)(2,1)}, u32[]{:S(2)}) copy-start(bf16[1024,256]{1,0:T(8,128)(2,1)} %get-tuple-element.18.kv_all) | copy-start | bytes 1572868
  58.6 0.6 copy-start.4
  59.2 11.9 %copy-start.10 = (f32[16,8,128]{2,1,0:T(8,128)S(1)}, f32[16,8,128]{2,1,0:T(8,128)}, u32[]{:S(2)}) copy-start(f32[16,8,128]{2,1,0:T(8,128)} %get-tuple-element.17.dl_all) | copy-start | bytes 196612
  71.1 1.0 copy-start.3
  80.9 0.8 copy-start.1
  81.7 0.8 copy-start.2
  82.5 36.1 %copy-start.11 = (bf16[2048,256]{1,0:T(8,128)(2,1)S(1)}, bf16[2048,256]{1,0:T(8,128)(2,1)}, u32[]{:S(2)}) copy-start(bf16[2048,256]{1,0:T(8,128)(2,1)} %param.14) | copy-start | bytes 3145732
  119.6 1.1 copy-start.14
  121.1 1.2 copy-start.16
  138.3 2.1 %copy-start.17 = (bf16[4,16,32,128]{3,2,1,0:T(8,128)(2,1)S(1)}, bf16[4,16,32,128]{3,2,1,0:T(8,128)(2,1)}, u32[]{:S(2)}) copy-start(bf16[4,16,32,128]{3,2,1,0:T(8,128)(2,1)} %get-tuple-element.22) | copy-start | bytes 1572868

commit v2 on v0

v2 whole, which is shorter than its diff:
```python
import jax
import jax.numpy as jnp
from jax import lax
from jax.experimental import pallas as pl
from jax.experimental.pallas import tpu as pltpu
from jax.sharding import Mesh
from jax.sharding import PartitionSpec as P

HD = 128
EPS = 1e-06
SCALE = HD ** (-0.5)
NZ, NY, NX, NC = 16, 4, 4, 2
MESH = pl.DeviceIdType.MESH
F32 = jnp.float32
BF16 = jnp.bfloat16
NT = (((1,), (1,)), ((), ()))
NN = (((1,), (0,)), ((), ()))
MESSAGES = 128


def dot(a, b, dims=NN):
    return lax.dot_general(a, b, dims, preferred_element_type=F32)


def normed(matrix, gain):
    wide = matrix.astype(F32)
    inverse = lax.rsqrt(jnp.mean(wide * wide, axis=-1, keepdims=True) + EPS)
    return (wide * inverse * gain).astype(BF16)


def normed_back(matrix, gain, cotangent):
    wide = matrix.astype(F32)
    inverse = lax.rsqrt(jnp.mean(wide * wide, axis=-1, keepdims=True) + EPS)
    scaled = cotangent * gain
    along = jnp.mean(scaled * wide, axis=-1, keepdims=True)
    return scaled * inverse - wide * (inverse * inverse * inverse * along)


def kernel(target, source, tgain, sgain, w_query, w_key, w_value, attended, d_attended,
           d_target, d_source, d_w,
           tg, sr, wq, wk, wv, nt_t, kv_own, kv, qd, st, st_all, lt, mg, lg,
           s_scr, g_scr, pt, ut, kt, dq, dq_in, dkv, near1, near2, near3, near4,
           far, far_in, dw, dw_in, dw1, dw2, dn, dn_in, load_sem, send_sem, recv_sem):
    z = lax.axis_index("z")
    y = lax.axis_index("y")
    x = lax.axis_index("x")
    c = lax.axis_index("c")
    xh = x // 2
    xl = lax.rem(x, 2)
    mine = y * 4 + xl * 2 + c
    tp = x * 2 + c

    def zmod(v):
        return lax.rem(v + NZ, NZ)

    def at(dz=0, dy=0, dxl=0, dc=0, dh=0):
        x2 = lax.rem(xh + dh, 2) * 2 + lax.rem(xl + dxl, 2)
        return (zmod(z + dz), lax.rem(y + dy, NY), x2, lax.rem(c + dc, 2))

    def block(dy, dxl, dc):
        return lax.rem(y + dy + NY, NY) * 4 + lax.rem(xl + dxl, 2) * 2 + lax.rem(c + dc, 2)

    def rows_of(j, n=128):
        return pl.ds(pl.multiple_of(j * n, n), n)

    count = [0]
    pending = []

    def remote(src, dst, dev):
        k = count[0]
        count[0] += 1
        cp = pltpu.make_async_remote_copy(
            src_ref=src, dst_ref=dst, send_sem=send_sem.at[k], recv_sem=recv_sem.at[k],
            device_id=dev, device_id_type=MESH)
        cp.start()
        pending.append(cp)
        return cp

    loads = []
    for k, (a, b) in enumerate(((source, sr), (w_key, wk), (w_value, wv), (target, tg), (w_query, wq))):
        cp = pltpu.make_async_copy(a, b, load_sem.at[k])
        cp.start()
        loads.append(cp)

    offs = [(dy, dx, dc) for dy in (2, 1, 3, 0) for dx in (1, 0) for dc in (1, 0)][:-1]
    tps = [(dh, dx, dc) for dh in (1, 0) for dx in (1, 0) for dc in (1, 0)][:-1]
    peers = [at(dy=a, dxl=b, dc=d) for a, b, d in offs]
    peers += [at(dz=k) for k in range(1, 16)]
    peers += [at(dz=k, dh=1) for k in (4, 8, 12)]
    peers += [at(dh=1, dxl=a, dc=b) for a in (0, 1) for b in (0, 1)]
    barrier = pltpu.get_barrier_semaphore()
    for d in peers:
        pl.semaphore_signal(barrier, inc=1, device_id=d, device_id_type=MESH)

    loads[0].wait()
    ns = normed(sr[...], sgain[...])
    loads[1].wait()
    loads[2].wait()
    key = dot(ns, wk[...]).astype(BF16)
    value = dot(ns, wv[...]).astype(BF16)
    kv_own[0] = jnp.concatenate([key[:, :128], value[:, :128]], axis=1)
    kv_own[1] = jnp.concatenate([key[:, 128:], value[:, 128:]], axis=1)
    pl.semaphore_wait(barrier, len(peers))

    g1 = {}
    for k, dh in ((0, 1), (2, 0), (2, 1), (1, 0), (1, 1), (3, 0), (3, 1)):
        slot = (4 - k) % 4
        g1[slot, dh] = remote(kv_own.at[lax.rem(xh + dh, 2)],
                              kv.at[pl.ds(slot * 64 + dh * 32, 32), :], at(dz=4 * k, dh=dh))
    kv[0:32, :] = kv_own[xh]

    loads[3].wait()
    nt = normed(tg[...], tgain[...])
    loads[4].wait()
    query = dot(nt, wq[...]).astype(BF16)
    qd[0, rows_of(mine), :] = query
    qd[1, rows_of(mine), :] = d_attended[...]
    own_qd = qd.at[:, rows_of(mine), :]
    qsend = {}
    for dy, dx in ((2, 0), (2, 1), (1, 0), (3, 0), (1, 1), (3, 1), (0, 1)):
        qsend[dy, dx] = remote(own_qd, own_qd, at(dy=dy, dxl=dx))
    qpart = remote(own_qd, own_qd, at(dc=1))

    prod = d_attended[...].astype(F32) * attended[...].astype(F32)
    delta = jnp.sum(jnp.transpose(prod), axis=0, keepdims=True).astype(BF16).astype(F32)
    st[32:40, :] = jnp.broadcast_to(delta, (8, 128))
    nt_t[...] = jnp.transpose(nt)

    near = {}

    def chunk(g, k):
        return kv.at[pl.ds(g * 256 + k * 64, 64), :]

    def forward(k, steps):
        for d in steps:
            if d == -1:
                dst = chunk(1, k)
            elif d == 1:
                dst = chunk(2, k)
            elif d == -2:
                dst = chunk(3, k)
            else:
                dst = chunk(3, {0: 3, 3: 2}[k])
            near[k, d] = remote(chunk(0, k), dst, at(dz=d))

    g1[0, 1].wait_recv()
    forward(0, (1, -1, 2, -2))
    qfwd = []
    for (dy, dx), cp in list(qsend.items())[2:]:
        cp.wait_recv()
        r = qd.at[:, rows_of(block(-dy, dx, 0)), :]
        qfwd.append(remote(r, r, at(dc=1)))
    for k, steps in ((1, (-2, 1, -1)), (3, (2, 1, -1))):
        g1[k, 0].wait_recv()
        g1[k, 1].wait_recv()
        forward(k, steps)
    for (dy, dx), cp in list(qsend.items())[:2]:
        cp.wait_recv()
        r = qd.at[:, rows_of(block(-dy, dx, 0)), :]
        qfwd.append(remote(r, r, at(dc=1)))
    g1[2, 0].wait_recv()
    g1[2, 1].wait_recv()
    forward(2, (1, -1))
    qpart.wait_recv()
    for cp in qfwd:
        cp.wait_recv()

    def scores(g):
        def pair(p, carry):
            rows = rows_of(p, 256)
            blk = slice(g * 256, (g + 1) * 256)
            s = dot(kv[blk, :128], qd[0, rows, :], NT) * SCALE
            s_scr[blk, rows] = s
            m = jnp.max(s, axis=0, keepdims=True)
            mg[g:g + 1, rows] = m
            lg[g:g + 1, rows] = jnp.sum(jnp.exp(s - m), axis=0, keepdims=True)
            return carry
        lax.fori_loop(0, 8, pair, 0)

    def weights_back(g):
        def pair(p, carry):
            rows = rows_of(p, 256)
            blk = slice(g * 256, (g + 1) * 256)
            g_scr[blk, rows] = dot(kv[blk, 128:], qd[1, rows, :], NT)
            return carry
        lax.fori_loop(0, 8, pair, 0)
        kt[:, g * 256:(g + 1) * 256] = jnp.transpose(kv[g * 256:(g + 1) * 256, :128])

    scores(0)
    weights_back(0)
    for k in range(4):
        near[k, -1].wait_recv()
    scores(1)
    weights_back(1)
    for k in range(4):
        near[k, 1].wait_recv()
    scores(2)
    weights_back(2)
    for k, d in ((0, -2), (1, -2), (3, 2), (0, 2)):
        near[k, d].wait_recv()
    scores(3)

    m4 = mg[0:4, :]
    m1 = jnp.max(m4, axis=0, keepdims=True)
    l1 = jnp.sum(lg[0:4, :] * jnp.exp(m4 - m1), axis=0, keepdims=True)
    for j in range(16):
        st[j:j + 1, :] = m1[:, j * 128:(j + 1) * 128]
        st[j + 16:j + 17, :] = l1[:, j * 128:(j + 1) * 128]
    stats = [remote(st, st_all.at[mine], at(dy=a, dxl=b, dc=d)) for a, b, d in offs]
    st_all[mine] = st[...]
    weights_back(3)
    for cp in stats:
        cp.wait_recv()

    top = jnp.max(st_all[:, 0:16, :], axis=0)
    total = jnp.zeros((16, 128), F32)
    for j in range(16):
        total = total + st_all[j, 16:32, :] * jnp.exp(st_all[j, 0:16, :] - top)
    lt[...] = top + jnp.log(total)

    def grads(p, carry):
        rows = rows_of(p, 256)
        lrow = jnp.concatenate([lt[pl.ds(2 * p, 1), :], lt[pl.ds(2 * p + 1, 1), :]], axis=1)
        drow = jnp.concatenate([st_all[2 * p, 32:33, :], st_all[2 * p + 1, 32:33, :]], axis=1)
        for g in range(4):
            blk = slice(g * 256, (g + 1) * 256)
            w = jnp.exp(s_scr[blk, rows] - lrow)
            pt[blk, rows] = w.astype(BF16)
            ut[blk, rows] = (w * (g_scr[blk, rows] - drow)).astype(BF16)
        dqt = dot(kt[...], ut[:, rows]) * SCALE
        dq[rows, :] = jnp.transpose(dqt).astype(BF16)
        return carry

    lax.fori_loop(0, 8, grads, 0)
    dq_send = [remote(dq.at[rows_of(block(a, b, d)), :], dq_in.at[mine], at(dy=a, dxl=b, dc=d))
               for a, b, d in offs]
    dq_in[mine] = dq[rows_of(mine), :]

    def key_grads(g):
        blk = slice(g * 256, (g + 1) * 256)
        dk = dot(ut[blk, :], qd[0]) * SCALE
        dv = dot(pt[blk, :], qd[1])
        dkv[blk, :] = jnp.concatenate([dk, dv], axis=1).astype(BF16)

    key_grads(3)
    n3 = remote(dkv.at[pl.ds(768, 128), :], near3, at(dz=2))
    n4 = remote(dkv.at[pl.ds(896, 128), :], near4, at(dz=-2))
    key_grads(1)
    n1 = remote(dkv.at[pl.ds(256, 256), :], near1, at(dz=1))
    key_grads(2)
    n2 = remote(dkv.at[pl.ds(512, 256), :], near2, at(dz=-1))
    key_grads(0)

    for cp in dq_send:
        cp.wait_recv()
    acc = dq_in[0].astype(F32)
    for j in range(1, 16):
        acc = acc + dq_in[j].astype(F32)
    dqb = acc.astype(BF16)
    dw[...] = dot(nt_t[...], dqb).astype(BF16).reshape(16, 4, 32, 128)
    w_send = [remote(dw.at[:, lax.rem(y + d, NY)], dw_in.at[y], at(dy=d)) for d in (2, 1, 3)]
    dn[...] = dot(dqb, wq[...], NT).astype(BF16)
    n_send = []
    for a, b, d in tps:
        dev = at(dh=a, dxl=b, dc=d)
        n_send.append(remote(dn.at[rows_of(dev[2] * 2 + dev[3], 16), :], dn_in.at[tp], dev))
    dw_in[y] = dw[:, y]
    dn_in[tp] = dn[rows_of(tp, 16), :]

    for cp in (n3, n4, n1, n2):
        cp.wait_recv()
    base = near1[...].astype(F32) + near2[...].astype(F32) + dkv[0:256, :].astype(F32)
    x3 = near3[...].astype(F32)
    x4 = near4[...].astype(F32)
    far[0:64, :] = (base[0:64] + x3[0:64] + x4[64:128]).astype(BF16)
    far[64:128, :] = (base[64:128] + x3[64:128]).astype(BF16)
    far[128:192, :] = base[128:192].astype(BF16)
    far[192:256, :] = (base[192:256] + x4[0:64]).astype(BF16)
    f_send = []
    for k, dh in ((2, 0), (2, 1), (1, 0), (1, 1), (3, 0), (3, 1), (0, 1)):
        f_send.append(remote(far.at[pl.ds(k * 64 + dh * 32, 32), :], far_in.at[dh, k],
                             at(dz=4 * k, dh=dh)))
    far_in[0, 0] = far[0:32, :]

    for cp in w_send:
        cp.wait_recv()
    wsum = dw_in[0].astype(F32)
    for j in range(1, 4):
        wsum = wsum + dw_in[j].astype(F32)
    dw1[...] = wsum.astype(BF16)
    z_send = [remote(dw1.at[zmod(z + d)], dw2.at[z], at(dz=d))
              for d in (8, 7, 9, 6, 10, 5, 11, 4, 12, 3, 13, 2, 14, 1, 15)]
    dw2[z] = dw1[z]

    for cp in n_send:
        cp.wait_recv()
    nsum = dn_in[0].astype(F32)
    for j in range(1, 8):
        nsum = nsum + dn_in[j].astype(F32)
    d_target[rows_of(tp, 16), :] = normed_back(tg[rows_of(tp, 16), :], tgain[...], nsum).astype(BF16)
    own_t = d_target.at[rows_of(tp, 16), :]
    t_send = [remote(own_t, own_t, at(dh=a, dxl=b, dc=d)) for a, b, d in tps]

    for cp in f_send:
        cp.wait_recv()
    fs = []
    for dh in range(2):
        v = far_in[dh, 0].astype(F32)
        for k in range(1, 4):
            v = v + far_in[dh, k].astype(F32)
        fs.append(v)
    low = jnp.where(xh == 0, fs[0], fs[1]).astype(BF16)
    high = jnp.where(xh == 0, fs[1], fs[0]).astype(BF16)
    dkey = jnp.concatenate([low[:, :128], high[:, :128]], axis=1)
    dval = jnp.concatenate([low[:, 128:], high[:, 128:]], axis=1)
    dns = dot(dkey, wk[...], NT) + dot(dval, wv[...], NT)
    d_source[...] = normed_back(sr[...], sgain[...], dns)

    for cp in z_send:
        cp.wait_recv()
    zsum = dw2[0].astype(F32)
    for j in range(1, 16):
        zsum = zsum + dw2[j].astype(F32)
    d_w[...] = zsum
    for cp in t_send:
        cp.wait_recv()
    for cp in pending:
        cp.wait_send()


def local(target, source, target_gain, source_gain, w_query, w_key, w_value, attended, d_attended):
    vm = pl.BlockSpec(memory_space=pltpu.VMEM)
    anywhere = pl.BlockSpec(memory_space=pl.ANY)
    v = pltpu.VMEM
    return pl.pallas_call(
        kernel,
        out_shape=[jax.ShapeDtypeStruct((128, 2048), BF16), jax.ShapeDtypeStruct((32, 2048), F32),
                   jax.ShapeDtypeStruct((32, 128), F32)],
        in_specs=[anywhere, anywhere, vm, vm, anywhere, anywhere, anywhere, vm, vm],
        out_specs=[vm, vm, vm],
        scratch_shapes=[
            v((128, 2048), BF16), v((32, 2048), BF16), v((2048, 128), BF16),
            v((2048, 256), BF16), v((2048, 256), BF16), v((2048, 128), BF16),
            v((2, 32, 256), BF16), v((1024, 256), BF16), v((2, 2048, 128), BF16),
            v((40, 128), F32), v((16, 40, 128), F32), v((16, 128), F32),
            v((8, 2048), F32), v((8, 2048), F32),
            v((1024, 2048), F32), v((1024, 2048), F32),
            v((1024, 2048), BF16), v((1024, 2048), BF16), v((128, 1024), BF16),
            v((2048, 128), BF16), v((16, 128, 128), BF16), v((1024, 256), BF16),
            v((256, 256), BF16), v((256, 256), BF16), v((128, 256), BF16), v((128, 256), BF16),
            v((256, 256), BF16), v((2, 4, 32, 256), BF16),
            v((16, 4, 32, 128), BF16), v((4, 16, 32, 128), BF16), v((16, 32, 128), BF16),
            v((16, 32, 128), BF16), v((128, 2048), BF16), v((8, 16, 2048), BF16),
            pltpu.SemaphoreType.DMA((5,)), pltpu.SemaphoreType.DMA((MESSAGES,)),
            pltpu.SemaphoreType.DMA((MESSAGES,)),
        ],
        compiler_params=pltpu.CompilerParams(
            collective_id=0, has_side_effects=True, vmem_limit_bytes=56 * 1024 * 1024),
        name="step",
    )(target, source, target_gain.reshape(1, 2048), source_gain.reshape(1, 2048),
      w_query, w_key, w_value, attended, d_attended)


def solution(mesh):
    fine = Mesh(mesh.devices.reshape(NZ, NY, NX, NC), ("z", "y", "x", "c"))
    sp = ("z", "y")
    tp = ("x", "c")
    both = ("z", "y", "x", "c")
    placed = (P(sp, None), P(both, None), P(), P(), P(None, tp), P(), P(), P(sp, tp), P(sp, tp))
    return jax.shard_map(
        local, mesh=fine, in_specs=placed,
        out_specs=(P(sp, None), P(both, None), P(sp, tp)), check_vma=False)
```

time: 664 us -> 86.6 us (0.13); the launches traced: 656 us -> 86.3 us
  waiting for transfers between devices: 299 us -> 0 us
  matrix products: 167 us -> 0 us
  blocking collectives: 88 us -> 0 us
  Pallas kernels: 0 us -> 82.4 us
  starting transfers between devices: 31 us -> 0 us
  local copies, waits for them, and re-layouts: 29.6 us -> 3.25 us
  other arithmetic: 25.7 us -> 0 us
  between operations: 14.2 us -> 0.65 us
    all_gather x3 -> x0, waiting for transfers between devices: 231 us -> none  [the longest x2 120 us: sent_together(): result = lax.all_gather(both, axis, axis=dim, tiled=True)]
    dot_general x135 -> x0, matrix products: 167 us -> none  [the longest x48 53.7 us: score_grads(): jnp.einsum('rhd,sd->rhs', query_heads, key_head, preferred_element_type=j...]
    all_gather x5 -> x0, blocking collectives: 88 us -> none  [the longest x4 68.5 us: joined_all(): pieces = jax.tree.map(lambda part: lax.all_gather(part, axis), shard)]
    pallas_call x0 -> x1, Pallas kernels: none -> 82.4 us  [local(): pl.pallas_call(kernel, out_shape=[jax.ShapeDtypeStruct((128, 2048), BF16)...]
    all_to_all x4 -> x0, waiting for transfers between devices: 67.4 us -> none  [the longest x1 48.5 us: sent_and_summed(): lax.all_to_all(pieces, axis, split_axis=0, concat_axis=0, tiled=True)]
    all_to_all x4 -> x0, starting transfers between devices: 30.9 us -> none  [the longest x1 12.7 us: summed_on_arrival(): lax.all_to_all(in_blocks(shard, dim, peers), axis, 0, 0, tiled=True)]
    convert_element_type x50 -> x0, other arithmetic: 13.4 us -> none  [the longest x48 11.5 us: score_grads(): delta_rows.astype(jnp.float32)[..., None]]
    split x4 -> x0, local copies, waits for them, and re-layouts: 11 us -> none  [sent_together(): jnp.split(result, [sum(widths[:k]) for k in range(1, len(widths))], axis=...]
  transfers between devices with their start and end apart: 7 -> 0, of which waited for: 7 -> 0; matrix products, arithmetic and copies ran while one was open for 19% -> 0% of each run, Pallas kernels for 0% -> 0%
where the time goes in v2:
time: 86.6 us; the launch traced here: 86.3 us
  Pallas kernels  82.4 us (95%)
  local copies, waits for them, and re-layouts  3.25 us (4%)
    pallas_call x1, Pallas kernels, local(): pl.pallas_call(kernel, out_shape=[jax.ShapeDtypeStruct((128, 2048), BF16)...  82.4 us
    unnamed x7, local copies, waits for them, and re-layouts  3.25 us

profile of v2, /device:TPU:1, one launch (start us, length us, event | category | flops | bytes accessed | tf_op | source)
XLA Modules:
  0.0 86.3 jit_solution(16107845500117454656)
XLA Ops:
  0.6 82.4 %step.1 = (bf16[128,2048]{1,0:T(8,128)(2,1)}, f32[32,2048]{1,0:T(8,128)}, f32[32,128]{1,0:T(8,128)}) custom-call(bf16[128,2048]{1,0:T(8,128)(2,1)} %target.1, bf16[32,2048]{1,0:T(8,128)(2,1)} %source.1, f32[1,2048]{1,0:T(1,128)} %bitcast.2, f32[1,2048]{1,0:T(1,128)} %bitcast.3, bf16[2048,128]{1,0:T(8,128)(2,1)} %w_query.1, bf16[2048,256]{1,0:T(8,128)(2,1)} %w_key.1, ...), custom_call_target="tpu_custom_call" | custom-call | tf_op jit(solution)/shard_map/step/pallas_call | solution.py:335
  83.1 0.0 copy-start
  83.1 1.9 %copy.15 = bf16[128,2048]{1,0:T(8,128)(2,1)} copy(bf16[128,2048]{1,0:T(8,128)(2,1)} %get-tuple-element.6) | data formatting | bytes 1048576
  85.0 0.0 copy-done
  85.0 0.0 copy-start.1
  85.0 0.7 copy.16
  85.7 0.0 copy-done.1
  85.7 0.6 copy.17
Async XLA Ops:
  83.1 1.9 %copy-start = (f32[32,2048]{1,0:T(8,128)S(1)}, f32[32,2048]{1,0:T(8,128)}, u32[]{:S(2)}) copy-start(f32[32,2048]{1,0:T(8,128)} %get-tuple-element.7) | copy-start | bytes 786436
  85.0 0.7 copy-start.1

commit v3 on v2

v3 whole, which is shorter than its diff:
```python
import jax
import jax.numpy as jnp
from jax import lax
from jax.experimental import pallas as pl
from jax.experimental.pallas import tpu as pltpu
from jax.sharding import Mesh
from jax.sharding import PartitionSpec as P

HD = 128
EPS = 1e-06
SCALE = HD ** (-0.5)
LOG2E = 1.4426950408889634
NZ, NY, NX, NC = 16, 4, 4, 2
MESH = pl.DeviceIdType.MESH
F32 = jnp.float32
BF16 = jnp.bfloat16
NT = (((1,), (1,)), ((), ()))
NN = (((1,), (0,)), ((), ()))
MESSAGES = 208
BASE = {0: 0, 1: 320, 3: 576, 2: 832}
SIZE = {0: 320, 1: 256, 3: 256, 2: 192}
NEAR = {0: (1, -1, 2, -2), 1: (-2, 1, -1), 3: (2, 1, -1), 2: (1, -1)}
ZORDER = (8, 7, 9, 6, 10, 5, 11, 4, 12, 3, 13, 2, 14, 1, 15, 0)


def dot(a, b, dims=NN):
    return lax.dot_general(a, b, dims, preferred_element_type=F32)


def place(k, d):
    if d == 0:
        slot = 0
    elif d == -1:
        slot = 1
    elif d == 1:
        slot = 2
    elif d == -2:
        slot = 3
    else:
        slot = 4 if k == 0 else 3
    return BASE[k] + 64 * slot


def normed(matrix, gain):
    wide = matrix.astype(F32)
    inverse = lax.rsqrt(jnp.mean(wide * wide, axis=-1, keepdims=True) + EPS)
    return (wide * inverse * gain).astype(BF16)


def normed_back(matrix, gain, cotangent):
    wide = matrix.astype(F32)
    inverse = lax.rsqrt(jnp.mean(wide * wide, axis=-1, keepdims=True) + EPS)
    scaled = cotangent * gain
    along = jnp.mean(scaled * wide, axis=-1, keepdims=True)
    return scaled * inverse - wide * (inverse * inverse * inverse * along)


def kernel(target, source, tgain, sgain, w_query, w_key, w_value, attended, d_attended,
           d_target, d_source, d_w,
           tg, sr, wq, wk, wv, tgn, sgn, att, dat, nt_t, kv_own, kv, q, do, dl, own_dl,
           st, st_all, mg, lg, e_scr, u_scr, pt, ut, kt, dqf, dq, dq_in, q_t, do_t, q2, do2, dkv, near_in,
           far, far_in, dw, dw_in, dw1, dw2, dn, dn_pair, dn2, dn_in,
           load_sem, send_sem, recv_sem):
    z = lax.axis_index("z")
    y = lax.axis_index("y")
    x = lax.axis_index("x")
    c = lax.axis_index("c")
    xh = x // 2
    xl = lax.rem(x, 2)
    mine = y * 4 + xl * 2 + c
    tp = x * 2 + c

    def zmod(v):
        return lax.rem(v + NZ, NZ)

    def at(dz=0, dy=0, dxl=0, dc=0, dh=0):
        x2 = lax.rem(xh + dh, 2) * 2 + lax.rem(xl + dxl, 2)
        return (zmod(z + dz), lax.rem(y + dy, NY), x2, lax.rem(c + dc, 2))

    def block(dy, dxl, dc):
        return lax.rem(y + dy + NY, NY) * 4 + lax.rem(xl + dxl, 2) * 2 + lax.rem(c + dc, 2)

    def rows_of(j, n=128):
        return pl.ds(pl.multiple_of(j * n, n), n)

    count = [0]
    pending = []

    def remote(src, dst, dev):
        k = count[0]
        count[0] += 1
        cp = pltpu.make_async_remote_copy(
            src_ref=src, dst_ref=dst, send_sem=send_sem.at[k], recv_sem=recv_sem.at[k],
            device_id=dev, device_id_type=MESH)
        cp.start()
        pending.append(cp)
        return cp

    loads = []
    for k, (a, b) in enumerate(((source, sr), (sgain, sgn), (w_key, wk), (w_value, wv),
                                (target, tg), (tgain, tgn), (w_query, wq),
                                (d_attended, dat), (attended, att))):
        cp = pltpu.make_async_copy(a, b, load_sem.at[k])
        cp.start()
        loads.append(cp)

    offs = [(dy, dx, dc) for dy in (2, 1, 3, 0) for dx in (1, 0) for dc in (1, 0)][:-1]
    peers = [at(dy=a, dxl=b, dc=d) for a, b, d in offs]
    peers += [at(dz=k) for k in range(1, 16)]
    peers += [at(dz=k, dh=1) for k in (4, 8, 12)]
    peers += [at(dh=1, dxl=a, dc=b) for a in (0, 1) for b in (0, 1)]
    barrier = pltpu.get_barrier_semaphore()
    for d in peers:
        pl.semaphore_signal(barrier, inc=1, device_id=d, device_id_type=MESH)

    for k in range(4):
        loads[k].wait()
    ns = normed(sr[...], sgn[...])
    key = dot(ns, wk[...]).astype(BF16)
    value = dot(ns, wv[...]).astype(BF16)
    kv_own[0] = jnp.concatenate([key[:, :128], value[:, :128]], axis=1)
    kv_own[1] = jnp.concatenate([key[:, 128:], value[:, 128:]], axis=1)
    pl.semaphore_wait(barrier, len(peers))

    g1 = {}
    for k, dh in ((0, 1), (2, 0), (2, 1), (1, 0), (1, 1), (3, 0), (3, 1)):
        slot = (4 - k) % 4
        g1[slot, dh] = remote(kv_own.at[lax.rem(xh + dh, 2)],
                              kv.at[pl.ds(place(slot, 0) + dh * 32, 32), :], at(dz=4 * k, dh=dh))
    kv[0:32, :] = kv_own[xh]

    for k in range(4, 9):
        loads[k].wait()
    nt = normed(tg[...], tgn[...])
    q[rows_of(mine), :] = dot(nt, wq[...]).astype(BF16)
    do[rows_of(mine), :] = dat[...]
    chips = ((2, 0), (2, 1), (1, 0), (3, 0), (1, 1), (3, 1), (0, 1))
    own_q = q.at[rows_of(mine), :]
    own_do = do.at[rows_of(mine), :]
    q_send = {o: remote(own_q, own_q, at(dy=o[0], dxl=o[1])) for o in chips}
    q_pair = remote(own_q, own_q, at(dc=1))
    prod = dat[...].astype(F32) * att[...].astype(F32)
    delta = jnp.sum(jnp.transpose(prod), axis=0, keepdims=True).astype(BF16).astype(F32)
    own_dl[...] = jnp.broadcast_to(delta, (8, 128))
    dl[mine] = own_dl[...]
    do_send = {o: remote(own_do, own_do, at(dy=o[0], dxl=o[1])) for o in chips}
    do_pair = remote(own_do, own_do, at(dc=1))
    dl_send = [remote(own_dl, dl.at[mine], at(dy=a, dxl=b, dc=d)) for a, b, d in offs]
    nt_t[...] = jnp.transpose(nt)

    near = {}

    def forward(k):
        src = kv.at[pl.ds(place(k, 0), 64), :]
        for d in NEAR[k]:
            near[k, d] = remote(src, kv.at[pl.ds(place(k, d), 64), :], at(dz=d))

    def pass_on(sends, array):
        out = []
        for dy, dx in ((0, 1), (1, 0), (3, 0), (1, 1), (3, 1), (2, 0), (2, 1)):
            sends[dy, dx].wait_recv()
            r = array.at[rows_of(block(-dy, dx, 0)), :]
            out.append(remote(r, r, at(dc=1)))
        return out

    def arrived(k):
        for d in NEAR[k]:
            near[k, d].wait_recv()

    def far_arrived(k):
        for dh in (0, 1):
            if (k, dh) != (0, 0):
                g1[k, dh].wait_recv()

    def scores(k):
        base, size = BASE[k], SIZE[k]

        def pair(p, carry):
            cols = rows_of(p, 256)
            s = dot(kv[base:base + size, :128], q_t[:, cols])
            for i in range(size // 64):
                t = s[i * 64:(i + 1) * 64].reshape(8, 8, 256) * (SCALE * LOG2E)
                m = jnp.max(t, axis=0)
                e = jnp.exp2(t - m[None])
                n = base // 64 + i
                mg[n, :, cols] = m
                lg[n, :, cols] = jnp.sum(e, axis=0)
                e_scr[base + i * 64:base + (i + 1) * 64, cols] = e.reshape(64, 256)
            return carry

        lax.fori_loop(0, 8, pair, 0, unroll=2)

    def weights_back(k):
        base, size = BASE[k], SIZE[k]

        def pair(p, carry):
            cols = rows_of(p, 256)
            g = dot(kv[base:base + size, 128:], do_t[:, cols])
            drow = jnp.concatenate([dl[2 * p, 0:1, :], dl[2 * p + 1, 0:1, :]], axis=1)
            u_scr[base:base + size, cols] = e_scr[base:base + size, cols] * (g - drow)
            return carry

        lax.fori_loop(0, 8, pair, 0, unroll=2)

    far_arrived(0)
    forward(0)
    q_fwd = pass_on(q_send, q)
    for k in (1, 3):
        far_arrived(k)
        forward(k)
    q_pair.wait_recv()
    for cp in q_fwd:
        cp.wait_recv()
    q_t[...] = jnp.transpose(q[...])
    arrived(0)
    scores(0)
    do_fwd = pass_on(do_send, do)
    arrived(1)
    scores(1)
    arrived(3)
    scores(3)
    far_arrived(2)
    forward(2)
    do_pair.wait_recv()
    for cp in do_fwd + dl_send:
        cp.wait_recv()
    do_t[...] = jnp.transpose(do[...])
    weights_back(0)
    kt[:, :832] = jnp.transpose(kv[:832, :128])
    arrived(2)
    scores(2)
    top8 = jnp.max(mg[...], axis=0)
    top1 = jnp.max(top8, axis=0, keepdims=True)
    tot = lg[0] * jnp.exp2(mg[0] - top1)
    for i in range(1, 16):
        tot = tot + lg[i] * jnp.exp2(mg[i] - top1)
    lse = top1 + jnp.log(jnp.sum(tot, axis=0, keepdims=True)) * LOG2E
    for j in range(16):
        st[j:j + 1, :] = lse[:, j * 128:(j + 1) * 128]
    stats = [remote(st, st_all.at[mine], at(dy=a, dxl=b, dc=d)) for a, b, d in offs]
    st_all[mine] = st[...]
    for i in range(16):
        mg[i] = jnp.exp2(mg[i] - lse)
    weights_back(1)
    weights_back(3)
    weights_back(2)
    kt[:, 832:] = jnp.transpose(kv[832:, :128])

    def grads(p, carry):
        cols = rows_of(p, 256)
        for i in range(16):
            r = slice(i * 64, (i + 1) * 64)
            f = mg[i, :, cols][None]
            pt[r, cols] = (e_scr[r, cols].reshape(8, 8, 256) * f).reshape(64, 256).astype(BF16)
            ut[r, cols] = (u_scr[r, cols].reshape(8, 8, 256) * f).reshape(64, 256).astype(BF16)
        dqf[cols, :] = jnp.transpose(dot(kt[...], ut[:, cols]) * SCALE)
        return carry

    lax.fori_loop(0, 8, grads, 0)
    for cp in stats:
        cp.wait_recv()
    top = jnp.max(st_all[...], axis=0)
    total = jnp.zeros((16, 128), F32)
    for j in range(16):
        total = total + jnp.exp2(st_all[j] - top)
    factor = jnp.exp2(st[...] - (top + jnp.log(total) * LOG2E))
    factor_t = jnp.transpose(jnp.concatenate([factor, jnp.zeros((112, 128), F32)], axis=0))
    for j in range(16):
        r = slice(j * 128, (j + 1) * 128)
        dq[r, :] = (dqf[r, :] * factor_t[:, j:j + 1]).astype(BF16)
    dq_send = [remote(dq.at[rows_of(block(a, b, d)), :], dq_in.at[mine], at(dy=a, dxl=b, dc=d))
               for a, b, d in offs]
    dq_in[mine] = dq[rows_of(mine), :]
    for j in range(16):
        r = slice(j * 128, (j + 1) * 128)
        f = factor_t[:, j:j + 1]
        q2[r, :] = (q[r, :].astype(F32) * f).astype(BF16)
        do2[r, :] = (do[r, :].astype(F32) * f).astype(BF16)
    back = {}
    index = 0
    for k in (2, 1, 3, 0):
        r = slice(BASE[k], BASE[k] + SIZE[k])
        dk = dot(ut[r, :], q2[...]) * SCALE
        dv = dot(pt[r, :], do2[...])
        dkv[r, :] = jnp.concatenate([dk, dv], axis=1).astype(BF16)
        for d in NEAR[k]:
            back[k, d] = (remote(dkv.at[pl.ds(place(k, d), 64), :], near_in.at[index], at(dz=-d)),
                          index)
            index += 1

    for cp in dq_send:
        cp.wait_recv()
    acc = dq_in[0].astype(F32)
    for j in range(1, 16):
        acc = acc + dq_in[j].astype(F32)
    dqb = acc.astype(BF16)
    w_all = dot(nt_t[...], dqb).astype(BF16)
    dn_all = dot(dqb, wq[...], NT).astype(BF16)
    dw[...] = w_all.reshape(16, 4, 32, 128)
    w_send = ([], [])
    for part in range(2):
        for d in (2, 1, 3):
            for i in range(8 * part, 8 * part + 8):
                w_send[part].append(remote(dw.at[zmod(z + ZORDER[i]), lax.rem(y + d, NY)],
                                           dw_in.at[i, y], at(dy=d)))
        if part == 0:
            dn[...] = dn_all.reshape(4, 2, 16, 2048)
            pair_send = remote(dn.at[:, lax.rem(c + 1, 2)], dn_pair, at(dc=1))
    for i in range(16):
        dw_in[i, y] = dw[zmod(z + ZORDER[i]), y]

    pair_send.wait_recv()
    dn2[...] = (dn[:, c].astype(F32) + dn_pair[...].astype(F32)).astype(BF16)
    n_send = []
    for a, b in ((1, 0), (1, 1), (0, 1)):
        dev = at(dh=a, dxl=b)
        n_send.append(remote(dn2.at[dev[2]], dn_in.at[x], dev))
    dn_in[x] = dn2[x]

    f_send = []
    for k in (2, 1, 3, 0):
        total_k = dkv[place(k, 0):place(k, 0) + 64, :].astype(F32)
        for d in NEAR[k]:
            cp, i = back[k, d]
            cp.wait_recv()
            total_k = total_k + near_in[i].astype(F32)
        far[k * 64:(k + 1) * 64, :] = total_k.astype(BF16)
        for dh in (0, 1):
            if (k, dh) != (0, 0):
                f_send.append(remote(far.at[pl.ds(k * 64 + dh * 32, 32), :], far_in.at[dh, k],
                                     at(dz=4 * k, dh=dh)))
    far_in[0, 0] = far[0:32, :]

    z_send = []
    for part in range(2):
        for cp in w_send[part]:
            cp.wait_recv()
        half = slice(8 * part, 8 * part + 8)
        wsum = dw_in[half, 0].astype(F32)
        for j in range(1, 4):
            wsum = wsum + dw_in[half, j].astype(F32)
        dw1[half] = wsum.astype(BF16)
        for i in range(8 * part, 8 * part + 8):
            if ZORDER[i]:
                z_send.append(remote(dw1.at[i], dw2.at[i], at(dz=ZORDER[i])))
    dw2[15] = dw1[15]

    for cp in n_send:
        cp.wait_recv()
    nsum = dn_in[0].astype(F32)
    for j in range(1, 4):
        nsum = nsum + dn_in[j].astype(F32)
    own_rows = rows_of(tp, 16)
    d_target[own_rows, :] = normed_back(tg[own_rows, :], tgn[...], nsum).astype(BF16)
    own_t = d_target.at[own_rows, :]
    t_send = {}
    for a, b in ((1, 0), (1, 1), (0, 1)):
        t_send[a, b] = remote(own_t, own_t, at(dh=a, dxl=b))
    t_pair = remote(own_t, own_t, at(dc=1))
    t_fwd = []
    for a, b in ((0, 1), (1, 0), (1, 1)):
        t_send[a, b].wait_recv()
        x2 = lax.rem(xh + a, 2) * 2 + lax.rem(xl + b, 2)
        r = d_target.at[rows_of(x2 * 2 + c, 16), :]
        t_fwd.append(remote(r, r, at(dc=1)))

    for cp in f_send:
        cp.wait_recv()
    fs = []
    for dh in range(2):
        v = far_in[dh, 0].astype(F32)
        for k in range(1, 4):
            v = v + far_in[dh, k].astype(F32)
        fs.append(v)
    low = jnp.where(xh == 0, fs[0], fs[1]).astype(BF16)
    high = jnp.where(xh == 0, fs[1], fs[0]).astype(BF16)
    dkey = jnp.concatenate([low[:, :128], high[:, :128]], axis=1)
    dval = jnp.concatenate([low[:, 128:], high[:, 128:]], axis=1)
    dns = dot(dkey, wk[...], NT) + dot(dval, wv[...], NT)
    d_source[...] = normed_back(sr[...], sgn[...], dns)

    for cp in z_send:
        cp.wait_recv()
    zsum = dw2[0].astype(F32)
    for j in range(1, 16):
        zsum = zsum + dw2[j].astype(F32)
    d_w[...] = zsum
    t_pair.wait_recv()
    for cp in t_fwd:
        cp.wait_recv()
    assert count[0] <= MESSAGES
    for cp in pending:
        cp.wait_send()


def store_kernel(a, b, w, a_out, b_out, w_out, sem):
    copies = [pltpu.make_async_copy(s, d, sem.at[k])
              for k, (s, d) in enumerate(((a, a_out), (b, b_out), (w, w_out)))]
    for cp in copies:
        cp.start()
    for cp in copies:
        cp.wait()


def local(target, source, target_gain, source_gain, w_query, w_key, w_value, attended, d_attended):
    vm = pl.BlockSpec(memory_space=pltpu.VMEM)
    anywhere = pl.BlockSpec(memory_space=pltpu.HBM)
    v = pltpu.VMEM
    outs = [jax.ShapeDtypeStruct((128, 2048), BF16), jax.ShapeDtypeStruct((32, 2048), F32),
            jax.ShapeDtypeStruct((32, 128), F32)]
    results = pl.pallas_call(
        kernel,
        out_shape=outs,
        in_specs=[anywhere] * 9,
        out_specs=[vm, vm, vm],
        scratch_shapes=[
            v((128, 2048), BF16), v((32, 2048), BF16), v((2048, 128), BF16),
            v((2048, 256), BF16), v((2048, 256), BF16), v((1, 2048), F32), v((1, 2048), F32),
            v((128, 128), BF16), v((128, 128), BF16), v((2048, 128), BF16),
            v((2, 32, 256), BF16), v((1024, 256), BF16), v((2048, 128), BF16), v((2048, 128), BF16),
            v((16, 8, 128), F32), v((8, 128), F32),
            v((16, 128), F32), v((16, 16, 128), F32), v((16, 8, 2048), F32), v((16, 8, 2048), F32),
            v((1024, 2048), F32), v((1024, 2048), F32),
            v((1024, 2048), BF16), v((1024, 2048), BF16), v((128, 1024), BF16),
            v((2048, 128), F32), v((2048, 128), BF16), v((16, 128, 128), BF16),
            v((128, 2048), BF16), v((128, 2048), BF16),
            v((2048, 128), BF16), v((2048, 128), BF16), v((1024, 256), BF16),
            v((12, 64, 256), BF16), v((256, 256), BF16), v((2, 4, 32, 256), BF16),
            v((16, 4, 32, 128), BF16), v((16, 4, 32, 128), BF16), v((16, 32, 128), BF16),
            v((16, 32, 128), BF16), v((4, 2, 16, 2048), BF16), v((4, 16, 2048), BF16),
            v((4, 16, 2048), BF16), v((4, 16, 2048), BF16),
            pltpu.SemaphoreType.DMA((9,)), pltpu.SemaphoreType.DMA((MESSAGES,)),
            pltpu.SemaphoreType.DMA((MESSAGES,)),
        ],
        compiler_params=pltpu.CompilerParams(
            collective_id=0, has_side_effects=True, vmem_limit_bytes=52 * 1024 * 1024),
        name="step",
    )(*(pltpu.with_memory_space_constraint(array, pltpu.HBM) for array in (
        target, source, target_gain.reshape(1, 2048), source_gain.reshape(1, 2048),
        w_query, w_key, w_value, attended, d_attended)))
    return tuple(pl.pallas_call(
        store_kernel, out_shape=outs, in_specs=[vm] * 3, out_specs=[anywhere] * 3,
        scratch_shapes=[pltpu.SemaphoreType.DMA((3,))],
        compiler_params=pltpu.CompilerParams(vmem_limit_bytes=4 * 1024 * 1024),
        name="store")(*results))


def solution(mesh):
    fine = Mesh(mesh.devices.reshape(NZ, NY, NX, NC), ("z", "y", "x", "c"))
    sp = ("z", "y")
    tp = ("x", "c")
    both = ("z", "y", "x", "c")
    placed = (P(sp, None), P(both, None), P(), P(), P(None, tp), P(), P(), P(sp, tp), P(sp, tp))
    return jax.shard_map(
        local, mesh=fine, in_specs=placed,
        out_specs=(P(sp, None), P(both, None), P(sp, tp)), check_vma=False)
```

time: 86.6 us -> 74.5 us (0.86)
  Pallas kernels: 82.4 us -> 73.8 us
  local copies, waits for them, and re-layouts: 3.25 us -> 0 us
    pallas_call x1 -> x2, Pallas kernels: 82.4 us -> 73.8 us  [the longest x1 72.9 us: local(): pl.pallas_call(kernel, out_shape=outs, in_specs=[anywhere] * 9, out_specs...]
    unnamed x7 -> x0, local copies, waits for them, and re-layouts: 3.25 us -> none
where the time goes in v3:
time: 74.5 us; the launch traced here: 74.4 us
  Pallas kernels  73.8 us (99%)
    pallas_call x1, Pallas kernels, local(): pl.pallas_call(kernel, out_shape=outs, in_specs=[anywhere] * 9, out_specs...  72.9 us

profile of v3, /device:TPU:1, one launch (start us, length us, event | category | flops | bytes accessed | tf_op | source)
XLA Modules:
  0.0 74.4 jit_solution(14896274350298366995)
XLA Ops:
  0.6 72.9 %step.1 = (bf16[128,2048]{1,0:T(8,128)(2,1)S(1)}, f32[32,2048]{1,0:T(8,128)S(1)}, f32[32,128]{1,0:T(8,128)S(1)}) custom-call(bf16[128,2048]{1,0:T(8,128)(2,1)} %target.1, bf16[32,2048]{1,0:T(8,128)(2,1)} %source.1, f32[1,2048]{1,0:T(1,128)} %bitcast.2, f32[1,2048]{1,0:T(1,128)} %bitcast.3, bf16[2048,128]{1,0:T(8,128)(2,1)} %w_query.1, ...), custom_call_target="tpu_custom_call" | custom-call | tf_op jit(solution)/shard_map/step/pallas_call | solution.py:411
  73.5 0.9 %store.1 = (bf16[128,2048]{1,0:T(8,128)(2,1)}, f32[32,2048]{1,0:T(8,128)}, f32[32,128]{1,0:T(8,128)}) custom-call(bf16[128,2048]{1,0:T(8,128)(2,1)S(1)} %get-tuple-element.6.a, f32[32,2048]{1,0:T(8,128)S(1)} %get-tuple-element.7.b, f32[32,128]{1,0:T(8,128)S(1)} %get-tuple-element.8.w), custom_call_target="tpu_custom_call" | custom-call | tf_op jit(solution)/shard_map/store/pallas_call | solution.py:441

commit v4 on v3

--- a/solution.py
+++ b/solution.py
@@ -16,7 +16,8 @@
 BF16 = jnp.bfloat16
 NT = (((1,), (1,)), ((), ()))
 NN = (((1,), (0,)), ((), ()))
-MESSAGES = 208
+MESSAGES = 160
+EARLY = 8
 BASE = {0: 0, 1: 320, 3: 576, 2: 832}
 SIZE = {0: 320, 1: 256, 3: 256, 2: 192}
 NEAR = {0: (1, -1, 2, -2), 1: (-2, 1, -1), 3: (2, 1, -1), 2: (1, -1)}
@@ -57,8 +58,8 @@
 
 def kernel(target, source, tgain, sgain, w_query, w_key, w_value, attended, d_attended,
            d_target, d_source, d_w,
-           tg, sr, wq, wk, wv, tgn, sgn, att, dat, nt_t, kv_own, kv, q, do, dl, own_dl,
-           st, st_all, mg, lg, e_scr, u_scr, pt, ut, kt, dqf, dq, dq_in, q_t, do_t, q2, do2, dkv, near_in,
+           tg, sr, wq, wk, wv, tgn, sgn, att, dat, nt_t, nt_r, kv_own, kv, q, do, dl, own_dl,
+           st, st_all, mg, lg, e_scr, u_scr, pt, ut, kt, dqf, frow, dq, dq_in, q_t, do_t, q2, do2, dkv, near_in,
            far, far_in, dw, dw_in, dw1, dw2, dn, dn_pair, dn2, dn_in,
            load_sem, send_sem, recv_sem):
     z = lax.axis_index("z")
@@ -147,6 +148,8 @@
     do_pair = remote(own_do, own_do, at(dc=1))
     dl_send = [remote(own_dl, dl.at[mine], at(dy=a, dxl=b, dc=d)) for a, b, d in offs]
     nt_t[...] = jnp.transpose(nt)
+    for i in range(16):
+        nt_r[i * 128:(i + 1) * 128, :] = nt_t[rows_of(zmod(z + ZORDER[i])), :]
 
     near = {}
 
@@ -175,8 +178,8 @@
     def scores(k):
         base, size = BASE[k], SIZE[k]
 
-        def pair(p, carry):
-            cols = rows_of(p, 256)
+        def pair(p):
+            cols = slice(p * 256, (p + 1) * 256)
             s = dot(kv[base:base + size, :128], q_t[:, cols])
             for i in range(size // 64):
                 t = s[i * 64:(i + 1) * 64].reshape(8, 8, 256) * (SCALE * LOG2E)
@@ -186,21 +189,21 @@
                 mg[n, :, cols] = m
                 lg[n, :, cols] = jnp.sum(e, axis=0)
                 e_scr[base + i * 64:base + (i + 1) * 64, cols] = e.reshape(64, 256)
-            return carry
-
-        lax.fori_loop(0, 8, pair, 0, unroll=2)
+
+        for p in range(8):
+            pair(p)
 
     def weights_back(k):
         base, size = BASE[k], SIZE[k]
 
-        def pair(p, carry):
-            cols = rows_of(p, 256)
+        def pair(p):
+            cols = slice(p * 256, (p + 1) * 256)
             g = dot(kv[base:base + size, 128:], do_t[:, cols])
             drow = jnp.concatenate([dl[2 * p, 0:1, :], dl[2 * p + 1, 0:1, :]], axis=1)
             u_scr[base:base + size, cols] = e_scr[base:base + size, cols] * (g - drow)
-            return carry
-
-        lax.fori_loop(0, 8, pair, 0, unroll=2)
+
+        for p in range(8):
+            pair(p)
 
     far_arrived(0)
     forward(0)
@@ -215,17 +218,18 @@
     arrived(0)
     scores(0)
     do_fwd = pass_on(do_send, do)
+    far_arrived(2)
+    forward(2)
     arrived(1)
     scores(1)
     arrived(3)
     scores(3)
-    far_arrived(2)
-    forward(2)
     do_pair.wait_recv()
     for cp in do_fwd + dl_send:
         cp.wait_recv()
     do_t[...] = jnp.transpose(do[...])
     weights_back(0)
+    weights_back(1)
     kt[:, :832] = jnp.transpose(kv[:832, :128])
     arrived(2)
     scores(2)
@@ -241,22 +245,45 @@
     st_all[mine] = st[...]
     for i in range(16):
         mg[i] = jnp.exp2(mg[i] - lse)
-    weights_back(1)
-    weights_back(3)
-    weights_back(2)
     kt[:, 832:] = jnp.transpose(kv[832:, :128])
 
-    def grads(p, carry):
+    def grads(dy, dx):
+        p = lax.rem(y + dy, NY) * 2 + lax.rem(xl + dx, 2)
         cols = rows_of(p, 256)
-        for i in range(16):
-            r = slice(i * 64, (i + 1) * 64)
-            f = mg[i, :, cols][None]
-            pt[r, cols] = (e_scr[r, cols].reshape(8, 8, 256) * f).reshape(64, 256).astype(BF16)
-            ut[r, cols] = (u_scr[r, cols].reshape(8, 8, 256) * f).reshape(64, 256).astype(BF16)
-        dqf[cols, :] = jnp.transpose(dot(kt[...], ut[:, cols]) * SCALE)
-        return carry
-
-    lax.fori_loop(0, 8, grads, 0)
+        drow = jnp.concatenate([dl[2 * p, 0:1, :], dl[2 * p + 1, 0:1, :]], axis=1)
+        dot_p = do_t[:, cols]
+        for k in (0, 1, 3, 2):
+            base, size = BASE[k], SIZE[k]
+            if k in (3, 2):
+                g = dot(kv[base:base + size, 128:], dot_p) - drow
+            for i in range(size // 64):
+                n = base // 64 + i
+                r = slice(n * 64, (n + 1) * 64)
+                f = mg[n, :, cols][None]
+                w = e_scr[r, cols].reshape(8, 8, 256) * f
+                pt[r, cols] = w.reshape(64, 256).astype(BF16)
+                if k in (3, 2):
+                    u = w * g[i * 64:(i + 1) * 64].reshape(8, 8, 256)
+                else:
+                    u = u_scr[r, cols].reshape(8, 8, 256) * f
+                ut[r, cols] = u.reshape(64, 256).astype(BF16)
+        return cols, dot(kt[...], ut[:, cols]) * SCALE
+
+    order = ((2, 1), (2, 0), (1, 1), (3, 1), (1, 0), (3, 0), (0, 1), (0, 0))
+    dq_send = []
+
+    def dq_out(cols, value, dy, dx):
+        dq[cols, :] = jnp.transpose(value * frow[0:1, cols]).astype(BF16)
+        for dc in (1, 0):
+            if (dy, dx, dc) != (0, 0, 0):
+                dq_send.append(remote(dq.at[rows_of(block(dy, dx, dc)), :], dq_in.at[mine],
+                                      at(dy=dy, dxl=dx, dc=dc)))
+
+    held = []
+    for dy, dx in order[:EARLY]:
+        cols, value = grads(dy, dx)
+        dqf[:, cols] = value
+        held.append((cols, dy, dx))
     for cp in stats:
         cp.wait_recv()
     top = jnp.max(st_all[...], axis=0)
@@ -266,10 +293,12 @@
     factor = jnp.exp2(st[...] - (top + jnp.log(total) * LOG2E))
     factor_t = jnp.transpose(jnp.concatenate([factor, jnp.zeros((112, 128), F32)], axis=0))
     for j in range(16):
-        r = slice(j * 128, (j + 1) * 128)
-        dq[r, :] = (dqf[r, :] * factor_t[:, j:j + 1]).astype(BF16)
-    dq_send = [remote(dq.at[rows_of(block(a, b, d)), :], dq_in.at[mine], at(dy=a, dxl=b, dc=d))
-               for a, b, d in offs]
+        frow[0:1, j * 128:(j + 1) * 128] = factor[j:j + 1, :]
+    for cols, dy, dx in held:
+        dq_out(cols, dqf[:, cols], dy, dx)
+    for dy, dx in order[EARLY:]:
+        cols, value = grads(dy, dx)
+        dq_out(cols, value, dy, dx)
     dq_in[mine] = dq[rows_of(mine), :]
     for j in range(16):
         r = slice(j * 128, (j + 1) * 128)
@@ -294,20 +323,19 @@
     for j in range(1, 16):
         acc = acc + dq_in[j].astype(F32)
     dqb = acc.astype(BF16)
-    w_all = dot(nt_t[...], dqb).astype(BF16)
+    w_all = dot(nt_r[...], dqb).astype(BF16)
     dn_all = dot(dqb, wq[...], NT).astype(BF16)
     dw[...] = w_all.reshape(16, 4, 32, 128)
     w_send = ([], [])
     for part in range(2):
         for d in (2, 1, 3):
-            for i in range(8 * part, 8 * part + 8):
-                w_send[part].append(remote(dw.at[zmod(z + ZORDER[i]), lax.rem(y + d, NY)],
-                                           dw_in.at[i, y], at(dy=d)))
+            some = pl.ds(8 * part, 8)
+            w_send[part].append(remote(dw.at[some, lax.rem(y + d, NY)], dw_in.at[some, y],
+                                       at(dy=d)))
         if part == 0:
             dn[...] = dn_all.reshape(4, 2, 16, 2048)
             pair_send = remote(dn.at[:, lax.rem(c + 1, 2)], dn_pair, at(dc=1))
-    for i in range(16):
-        dw_in[i, y] = dw[zmod(z + ZORDER[i]), y]
+    dw_in[:, y] = dw[:, y]
 
     pair_send.wait_recv()
     dn2[...] = (dn[:, c].astype(F32) + dn_pair[...].astype(F32)).astype(BF16)
@@ -332,7 +360,8 @@
     far_in[0, 0] = far[0:32, :]
 
     z_send = []
-    for part in range(2):
+
+    def z_part(part):
         for cp in w_send[part]:
             cp.wait_recv()
         half = slice(8 * part, 8 * part + 8)
@@ -343,6 +372,9 @@
         for i in range(8 * part, 8 * part + 8):
             if ZORDER[i]:
                 z_send.append(remote(dw1.at[i], dw2.at[i], at(dz=ZORDER[i])))
+
+    z_part(0)
+    z_part(1)
     dw2[15] = dw1[15]
 
     for cp in n_send:
@@ -416,13 +448,14 @@
         scratch_shapes=[
             v((128, 2048), BF16), v((32, 2048), BF16), v((2048, 128), BF16),
             v((2048, 256), BF16), v((2048, 256), BF16), v((1, 2048), F32), v((1, 2048), F32),
-            v((128, 128), BF16), v((128, 128), BF16), v((2048, 128), BF16),
+            v((128, 128), BF16), v((128, 128), BF16), v((2048, 128), BF16), v((2048, 128), BF16),
             v((2, 32, 256), BF16), v((1024, 256), BF16), v((2048, 128), BF16), v((2048, 128), BF16),
             v((16, 8, 128), F32), v((8, 128), F32),
             v((16, 128), F32), v((16, 16, 128), F32), v((16, 8, 2048), F32), v((16, 8, 2048), F32),
             v((1024, 2048), F32), v((1024, 2048), F32),
             v((1024, 2048), BF16), v((1024, 2048), BF16), v((128, 1024), BF16),
-            v((2048, 128), F32), v((2048, 128), BF16), v((16, 128, 128), BF16),
+            v((128, 2048), F32), v((8, 2048), F32), v((2048, 128), BF16),
+            v((16, 128, 128), BF16),
             v((128, 2048), BF16), v((128, 2048), BF16),
             v((2048, 128), BF16), v((2048, 128), BF16), v((1024, 256), BF16),
             v((12, 64, 256), BF16), v((256, 256), BF16), v((2, 4, 32, 256), BF16),

time: 74.5 us -> 69.5 us (0.933)
  Pallas kernels: 73.8 us -> 68.7 us
    pallas_call x1, Pallas kernels: 72.9 us -> 67.8 us  [local(): pl.pallas_call(kernel, out_shape=outs, in_specs=[anywhere] * 9, out_specs...]
where the time goes in v4:
time: 69.5 us; the launch traced here: 69.4 us
  Pallas kernels  68.7 us (99%)
    pallas_call x1, Pallas kernels, local(): pl.pallas_call(kernel, out_shape=outs, in_specs=[anywhere] * 9, out_specs...  67.8 us

profile of v4, /device:TPU:1, one launch (start us, length us, event | category | flops | bytes accessed | tf_op | source)
XLA Modules:
  0.0 69.4 jit_solution(13474659255737612799)
XLA Ops:
  0.6 67.8 %step.1 = (bf16[128,2048]{1,0:T(8,128)(2,1)S(1)}, f32[32,2048]{1,0:T(8,128)S(1)}, f32[32,128]{1,0:T(8,128)S(1)}) custom-call(bf16[128,2048]{1,0:T(8,128)(2,1)} %target.1, bf16[32,2048]{1,0:T(8,128)(2,1)} %source.1, f32[1,2048]{1,0:T(1,128)} %bitcast.2, f32[1,2048]{1,0:T(1,128)} %bitcast.3, bf16[2048,128]{1,0:T(8,128)(2,1)} %w_query.1, ...), custom_call_target="tpu_custom_call" | custom-call | tf_op jit(solution)/shard_map/step/pallas_call | solution.py:443
  68.5 0.9 %store.1 = (bf16[128,2048]{1,0:T(8,128)(2,1)}, f32[32,2048]{1,0:T(8,128)}, f32[32,128]{1,0:T(8,128)}) custom-call(bf16[128,2048]{1,0:T(8,128)(2,1)S(1)} %get-tuple-element.6.a, f32[32,2048]{1,0:T(8,128)S(1)} %get-tuple-element.7.b, f32[32,128]{1,0:T(8,128)S(1)} %get-tuple-element.8.w), custom_call_target="tpu_custom_call" | custom-call | tf_op jit(solution)/shard_map/store/pallas_call | solution.py:474

commit v5 on v4

--- a/solution.py
+++ b/solution.py
@@ -16,7 +16,7 @@
 BF16 = jnp.bfloat16
 NT = (((1,), (1,)), ((), ()))
 NN = (((1,), (0,)), ((), ()))
-MESSAGES = 160
+MESSAGES = 176
 EARLY = 8
 BASE = {0: 0, 1: 320, 3: 576, 2: 832}
 SIZE = {0: 320, 1: 256, 3: 256, 2: 192}
@@ -58,7 +58,7 @@
 
 def kernel(target, source, tgain, sgain, w_query, w_key, w_value, attended, d_attended,
            d_target, d_source, d_w,
-           tg, sr, wq, wk, wv, tgn, sgn, att, dat, nt_t, nt_r, kv_own, kv, q, do, dl, own_dl,
+           tg, sr, wq, wk, wv, tgn, sgn, att, dat, nt_t, nt_r, k_own, v_own, ks, vs, q, do, dl, own_dl,
            st, st_all, mg, lg, e_scr, u_scr, pt, ut, kt, dqf, frow, dq, dq_in, q_t, do_t, q2, do2, dkv, near_in,
            far, far_in, dw, dw_in, dw1, dw2, dn, dn_pair, dn2, dn_in,
            load_sem, send_sem, recv_sem):
@@ -102,7 +102,8 @@
                                 (target, tg), (tgain, tgn), (w_query, wq),
                                 (d_attended, dat), (attended, att))):
         cp = pltpu.make_async_copy(a, b, load_sem.at[k])
-        cp.start()
+        if k < 4:
+            cp.start()
         loads.append(cp)
 
     offs = [(dy, dx, dc) for dy in (2, 1, 3, 0) for dx in (1, 0) for dc in (1, 0)][:-1]
@@ -116,19 +117,24 @@
 
     for k in range(4):
         loads[k].wait()
+    for cp in loads[4:]:
+        cp.start()
     ns = normed(sr[...], sgn[...])
     key = dot(ns, wk[...]).astype(BF16)
     value = dot(ns, wv[...]).astype(BF16)
-    kv_own[0] = jnp.concatenate([key[:, :128], value[:, :128]], axis=1)
-    kv_own[1] = jnp.concatenate([key[:, 128:], value[:, 128:]], axis=1)
+    for i in range(2):
+        k_own[i] = key[:, i * 128:(i + 1) * 128]
+        v_own[i] = value[:, i * 128:(i + 1) * 128]
     pl.semaphore_wait(barrier, len(peers))
 
     g1 = {}
-    for k, dh in ((0, 1), (2, 0), (2, 1), (1, 0), (1, 1), (3, 0), (3, 1)):
-        slot = (4 - k) % 4
-        g1[slot, dh] = remote(kv_own.at[lax.rem(xh + dh, 2)],
-                              kv.at[pl.ds(place(slot, 0) + dh * 32, 32), :], at(dz=4 * k, dh=dh))
-    kv[0:32, :] = kv_own[xh]
+    for which, own, full in ((0, k_own, ks), (1, v_own, vs)):
+        for k, dh in ((0, 1), (2, 0), (2, 1), (1, 0), (1, 1), (3, 0), (3, 1)):
+            slot = (4 - k) % 4
+            g1[which, slot, dh] = remote(own.at[lax.rem(xh + dh, 2)],
+                                         full.at[pl.ds(place(slot, 0) + dh * 32, 32), :],
+                                         at(dz=4 * k, dh=dh))
+        full[0:32, :] = own[xh]
 
     for k in range(4, 9):
         loads[k].wait()
@@ -153,10 +159,11 @@
 
     near = {}
 
-    def forward(k):
-        src = kv.at[pl.ds(place(k, 0), 64), :]
+    def forward(which, k):
+        full = vs if which else ks
+        src = full.at[pl.ds(place(k, 0), 64), :]
         for d in NEAR[k]:
-            near[k, d] = remote(src, kv.at[pl.ds(place(k, d), 64), :], at(dz=d))
+            near[which, k, d] = remote(src, full.at[pl.ds(place(k, d), 64), :], at(dz=d))
 
     def pass_on(sends, array):
         out = []
@@ -166,21 +173,22 @@
             out.append(remote(r, r, at(dc=1)))
         return out
 
-    def arrived(k):
+    def arrived(which, k):
         for d in NEAR[k]:
-            near[k, d].wait_recv()
-
-    def far_arrived(k):
+            near[which, k, d].wait_recv()
+
+    def relay(which, k):
         for dh in (0, 1):
             if (k, dh) != (0, 0):
-                g1[k, dh].wait_recv()
+                g1[which, k, dh].wait_recv()
+        forward(which, k)
 
     def scores(k):
         base, size = BASE[k], SIZE[k]
 
         def pair(p):
             cols = slice(p * 256, (p + 1) * 256)
-            s = dot(kv[base:base + size, :128], q_t[:, cols])
+            s = dot(ks[base:base + size, :], q_t[:, cols])
             for i in range(size // 64):
                 t = s[i * 64:(i + 1) * 64].reshape(8, 8, 256) * (SCALE * LOG2E)
                 m = jnp.max(t, axis=0)
@@ -198,40 +206,34 @@
 
         def pair(p):
             cols = slice(p * 256, (p + 1) * 256)
-            g = dot(kv[base:base + size, 128:], do_t[:, cols])
+            g = dot(vs[base:base + size, :], do_t[:, cols])
             drow = jnp.concatenate([dl[2 * p, 0:1, :], dl[2 * p + 1, 0:1, :]], axis=1)
             u_scr[base:base + size, cols] = e_scr[base:base + size, cols] * (g - drow)
 
         for p in range(8):
             pair(p)
 
-    far_arrived(0)
-    forward(0)
+    relay(0, 0)
     q_fwd = pass_on(q_send, q)
-    for k in (1, 3):
-        far_arrived(k)
-        forward(k)
+    relay(0, 1)
+    relay(0, 3)
+    relay(1, 0)
     q_pair.wait_recv()
     for cp in q_fwd:
         cp.wait_recv()
     q_t[...] = jnp.transpose(q[...])
-    arrived(0)
+    arrived(0, 0)
     scores(0)
+    relay(0, 2)
     do_fwd = pass_on(do_send, do)
-    far_arrived(2)
-    forward(2)
-    arrived(1)
+    relay(1, 1)
+    relay(1, 3)
+    arrived(0, 1)
     scores(1)
-    arrived(3)
+    arrived(0, 3)
     scores(3)
-    do_pair.wait_recv()
-    for cp in do_fwd + dl_send:
-        cp.wait_recv()
-    do_t[...] = jnp.transpose(do[...])
-    weights_back(0)
-    weights_back(1)
-    kt[:, :832] = jnp.transpose(kv[:832, :128])
-    arrived(2)
+    relay(1, 2)
+    arrived(0, 2)
     scores(2)
     top8 = jnp.max(mg[...], axis=0)
     top1 = jnp.max(top8, axis=0, keepdims=True)
@@ -245,7 +247,15 @@
     st_all[mine] = st[...]
     for i in range(16):
         mg[i] = jnp.exp2(mg[i] - lse)
-    kt[:, 832:] = jnp.transpose(kv[832:, :128])
+    kt[...] = jnp.transpose(ks[...])
+    do_pair.wait_recv()
+    for cp in do_fwd + dl_send:
+        cp.wait_recv()
+    do_t[...] = jnp.transpose(do[...])
+    for k in (0, 1, 3):
+        arrived(1, k)
+        weights_back(k)
+    arrived(1, 2)
 
     def grads(dy, dx):
         p = lax.rem(y + dy, NY) * 2 + lax.rem(xl + dx, 2)
@@ -254,15 +264,15 @@
         dot_p = do_t[:, cols]
         for k in (0, 1, 3, 2):
             base, size = BASE[k], SIZE[k]
-            if k in (3, 2):
-                g = dot(kv[base:base + size, 128:], dot_p) - drow
+            if k == 2:
+                g = dot(vs[base:base + size, :], dot_p) - drow
             for i in range(size // 64):
                 n = base // 64 + i
                 r = slice(n * 64, (n + 1) * 64)
                 f = mg[n, :, cols][None]
                 w = e_scr[r, cols].reshape(8, 8, 256) * f
                 pt[r, cols] = w.reshape(64, 256).astype(BF16)
-                if k in (3, 2):
+                if k == 2:
                     u = w * g[i * 64:(i + 1) * 64].reshape(8, 8, 256)
                 else:
                     u = u_scr[r, cols].reshape(8, 8, 256) * f
@@ -449,7 +459,8 @@
             v((128, 2048), BF16), v((32, 2048), BF16), v((2048, 128), BF16),
             v((2048, 256), BF16), v((2048, 256), BF16), v((1, 2048), F32), v((1, 2048), F32),
             v((128, 128), BF16), v((128, 128), BF16), v((2048, 128), BF16), v((2048, 128), BF16),
-            v((2, 32, 256), BF16), v((1024, 256), BF16), v((2048, 128), BF16), v((2048, 128), BF16),
+            v((2, 32, 128), BF16), v((2, 32, 128), BF16), v((1024, 128), BF16),
+            v((1024, 128), BF16), v((2048, 128), BF16), v((2048, 128), BF16),
             v((16, 8, 128), F32), v((8, 128), F32),
             v((16, 128), F32), v((16, 16, 128), F32), v((16, 8, 2048), F32), v((16, 8, 2048), F32),
             v((1024, 2048), F32), v((1024, 2048), F32),

time: 69.5 us -> 66.4 us (0.955)
  Pallas kernels: 68.7 us -> 65.6 us
    pallas_call x1, Pallas kernels: 67.8 us -> 64.7 us  [local(): pl.pallas_call(kernel, out_shape=outs, in_specs=[anywhere] * 9, out_specs...]
where the time goes in v5:
time: 66.4 us; the launch traced here: 66.2 us
  Pallas kernels  65.6 us (99%)
    pallas_call x1, Pallas kernels, local(): pl.pallas_call(kernel, out_shape=outs, in_specs=[anywhere] * 9, out_specs...  64.7 us

profile of v5, /device:TPU:1, one launch (start us, length us, event | category | flops | bytes accessed | tf_op | source)
XLA Modules:
  0.0 66.2 jit_solution(13682560295282275242)
XLA Ops:
  0.6 64.7 %step.1 = (bf16[128,2048]{1,0:T(8,128)(2,1)S(1)}, f32[32,2048]{1,0:T(8,128)S(1)}, f32[32,128]{1,0:T(8,128)S(1)}) custom-call(bf16[128,2048]{1,0:T(8,128)(2,1)} %target.1, bf16[32,2048]{1,0:T(8,128)(2,1)} %source.1, f32[1,2048]{1,0:T(1,128)} %bitcast.2, f32[1,2048]{1,0:T(1,128)} %bitcast.3, bf16[2048,128]{1,0:T(8,128)(2,1)} %w_query.1, ...), custom_call_target="tpu_custom_call" | custom-call | tf_op jit(solution)/shard_map/step/pallas_call | solution.py:453
  65.3 0.9 %store.1 = (bf16[128,2048]{1,0:T(8,128)(2,1)}, f32[32,2048]{1,0:T(8,128)}, f32[32,128]{1,0:T(8,128)}) custom-call(bf16[128,2048]{1,0:T(8,128)(2,1)S(1)} %get-tuple-element.6.a, f32[32,2048]{1,0:T(8,128)S(1)} %get-tuple-element.7.b, f32[32,128]{1,0:T(8,128)S(1)} %get-tuple-element.8.w), custom_call_target="tpu_custom_call" | custom-call | tf_op jit(solution)/shard_map/store/pallas_call | solution.py:485

commit v6 on v5

--- a/solution.py
+++ b/solution.py
@@ -59,7 +59,7 @@
 def kernel(target, source, tgain, sgain, w_query, w_key, w_value, attended, d_attended,
            d_target, d_source, d_w,
            tg, sr, wq, wk, wv, tgn, sgn, att, dat, nt_t, nt_r, k_own, v_own, ks, vs, q, do, dl, own_dl,
-           st, st_all, mg, lg, e_scr, u_scr, pt, ut, kt, dqf, frow, dq, dq_in, q_t, do_t, q2, do2, dkv, near_in,
+           st, st_all, mg, lg, e_scr, pt, ut, kt, dqf, frow, dq, dq_in, q_t, do_t, q2, do2, dkv, near_in, via_in,
            far, far_in, dw, dw_in, dw1, dw2, dn, dn_pair, dn2, dn_in,
            load_sem, send_sem, recv_sem):
     z = lax.axis_index("z")
@@ -115,11 +115,13 @@
     for d in peers:
         pl.semaphore_signal(barrier, inc=1, device_id=d, device_id_type=MESH)
 
-    for k in range(4):
-        loads[k].wait()
+    loads[0].wait()
+    loads[1].wait()
+    ns = normed(sr[...], sgn[...])
+    loads[2].wait()
+    loads[3].wait()
     for cp in loads[4:]:
         cp.start()
-    ns = normed(sr[...], sgn[...])
     key = dot(ns, wk[...]).astype(BF16)
     value = dot(ns, wv[...]).astype(BF16)
     for i in range(2):
@@ -201,17 +203,17 @@
         for p in range(8):
             pair(p)
 
-    def weights_back(k):
+    def finish(k, cols, p):
         base, size = BASE[k], SIZE[k]
-
-        def pair(p):
-            cols = slice(p * 256, (p + 1) * 256)
-            g = dot(vs[base:base + size, :], do_t[:, cols])
-            drow = jnp.concatenate([dl[2 * p, 0:1, :], dl[2 * p + 1, 0:1, :]], axis=1)
-            u_scr[base:base + size, cols] = e_scr[base:base + size, cols] * (g - drow)
-
-        for p in range(8):
-            pair(p)
+        drow = jnp.concatenate([dl[2 * p, 0:1, :], dl[2 * p + 1, 0:1, :]], axis=1)
+        g = dot(vs[base:base + size, :], do_t[:, cols]) - drow
+        for i in range(size // 64):
+            n = base // 64 + i
+            r = slice(n * 64, (n + 1) * 64)
+            w = e_scr[r, cols].reshape(8, 8, 256) * mg[n, :, cols][None]
+            pt[r, cols] = w.reshape(64, 256).astype(BF16)
+            u = w * g[i * 64:(i + 1) * 64].reshape(8, 8, 256)
+            ut[r, cols] = u.reshape(64, 256).astype(BF16)
 
     relay(0, 0)
     q_fwd = pass_on(q_send, q)
@@ -254,29 +256,14 @@
     do_t[...] = jnp.transpose(do[...])
     for k in (0, 1, 3):
         arrived(1, k)
-        weights_back(k)
+        for p in range(8):
+            finish(k, slice(p * 256, (p + 1) * 256), p)
     arrived(1, 2)
 
     def grads(dy, dx):
         p = lax.rem(y + dy, NY) * 2 + lax.rem(xl + dx, 2)
         cols = rows_of(p, 256)
-        drow = jnp.concatenate([dl[2 * p, 0:1, :], dl[2 * p + 1, 0:1, :]], axis=1)
-        dot_p = do_t[:, cols]
-        for k in (0, 1, 3, 2):
-            base, size = BASE[k], SIZE[k]
-            if k == 2:
-                g = dot(vs[base:base + size, :], dot_p) - drow
-            for i in range(size // 64):
-                n = base // 64 + i
-                r = slice(n * 64, (n + 1) * 64)
-                f = mg[n, :, cols][None]
-                w = e_scr[r, cols].reshape(8, 8, 256) * f
-                pt[r, cols] = w.reshape(64, 256).astype(BF16)
-                if k == 2:
-                    u = w * g[i * 64:(i + 1) * 64].reshape(8, 8, 256)
-                else:
-                    u = u_scr[r, cols].reshape(8, 8, 256) * f
-                ut[r, cols] = u.reshape(64, 256).astype(BF16)
+        finish(2, cols, p)
         return cols, dot(kt[...], ut[:, cols]) * SCALE
 
     order = ((2, 1), (2, 0), (1, 1), (3, 1), (1, 0), (3, 0), (0, 1), (0, 0))
@@ -336,13 +323,13 @@
     w_all = dot(nt_r[...], dqb).astype(BF16)
     dn_all = dot(dqb, wq[...], NT).astype(BF16)
     dw[...] = w_all.reshape(16, 4, 32, 128)
-    w_send = ([], [])
-    for part in range(2):
+    w_send = ([], [], [], [])
+    for part in range(4):
         for d in (2, 1, 3):
-            some = pl.ds(8 * part, 8)
+            some = pl.ds(4 * part, 4)
             w_send[part].append(remote(dw.at[some, lax.rem(y + d, NY)], dw_in.at[some, y],
                                        at(dy=d)))
-        if part == 0:
+        if part == 1:
             dn[...] = dn_all.reshape(4, 2, 16, 2048)
             pair_send = remote(dn.at[:, lax.rem(c + 1, 2)], dn_pair, at(dc=1))
     dw_in[:, y] = dw[:, y]
@@ -356,6 +343,12 @@
     dn_in[x] = dn2[x]
 
     f_send = []
+    via = {}
+
+    def far_out(k, dh):
+        f_send.append(remote(far.at[pl.ds(k * 64 + dh * 32, 32), :], far_in.at[dh, k],
+                             at(dz=4 * k, dh=dh)))
+
     for k in (2, 1, 3, 0):
         total_k = dkv[place(k, 0):place(k, 0) + 64, :].astype(F32)
         for d in NEAR[k]:
@@ -364,9 +357,11 @@
             total_k = total_k + near_in[i].astype(F32)
         far[k * 64:(k + 1) * 64, :] = total_k.astype(BF16)
         for dh in (0, 1):
-            if (k, dh) != (0, 0):
-                f_send.append(remote(far.at[pl.ds(k * 64 + dh * 32, 32), :], far_in.at[dh, k],
-                                     at(dz=4 * k, dh=dh)))
+            if k == 2:
+                via[dh] = remote(far.at[pl.ds(k * 64 + dh * 32, 32), :], via_in.at[dh],
+                                 at(dz=-4 if dh else 4))
+            elif (k, dh) not in ((0, 0), (1, 0), (3, 1)):
+                far_out(k, dh)
     far_in[0, 0] = far[0:32, :]
 
     z_send = []
@@ -374,17 +369,24 @@
     def z_part(part):
         for cp in w_send[part]:
             cp.wait_recv()
-        half = slice(8 * part, 8 * part + 8)
+        half = slice(4 * part, 4 * part + 4)
         wsum = dw_in[half, 0].astype(F32)
         for j in range(1, 4):
             wsum = wsum + dw_in[half, j].astype(F32)
         dw1[half] = wsum.astype(BF16)
-        for i in range(8 * part, 8 * part + 8):
+        for i in range(4 * part, 4 * part + 4):
             if ZORDER[i]:
                 z_send.append(remote(dw1.at[i], dw2.at[i], at(dz=ZORDER[i])))
 
     z_part(0)
     z_part(1)
+    for k, dh in ((1, 0), (3, 1)):
+        via[dh].wait_recv()
+        r = slice(k * 64 + dh * 32, k * 64 + dh * 32 + 32)
+        far[r, :] = (far[r, :].astype(F32) + via_in[dh].astype(F32)).astype(BF16)
+        far_out(k, dh)
+    z_part(2)
+    z_part(3)
     dw2[15] = dw1[15]
 
     for cp in n_send:
@@ -411,7 +413,7 @@
     fs = []
     for dh in range(2):
         v = far_in[dh, 0].astype(F32)
-        for k in range(1, 4):
+        for k in (1, 3):
             v = v + far_in[dh, k].astype(F32)
         fs.append(v)
     low = jnp.where(xh == 0, fs[0], fs[1]).astype(BF16)
@@ -421,6 +423,8 @@
     dns = dot(dkey, wk[...], NT) + dot(dval, wv[...], NT)
     d_source[...] = normed_back(sr[...], sgn[...], dns)
 
+    for cp in pending:
+        cp.wait_send()
     for cp in z_send:
         cp.wait_recv()
     zsum = dw2[0].astype(F32)
@@ -431,8 +435,6 @@
     for cp in t_fwd:
         cp.wait_recv()
     assert count[0] <= MESSAGES
-    for cp in pending:
-        cp.wait_send()
 
 
 def store_kernel(a, b, w, a_out, b_out, w_out, sem):
@@ -463,13 +465,13 @@
             v((1024, 128), BF16), v((2048, 128), BF16), v((2048, 128), BF16),
             v((16, 8, 128), F32), v((8, 128), F32),
             v((16, 128), F32), v((16, 16, 128), F32), v((16, 8, 2048), F32), v((16, 8, 2048), F32),
-            v((1024, 2048), F32), v((1024, 2048), F32),
+            v((1024, 2048), F32),
             v((1024, 2048), BF16), v((1024, 2048), BF16), v((128, 1024), BF16),
             v((128, 2048), F32), v((8, 2048), F32), v((2048, 128), BF16),
             v((16, 128, 128), BF16),
             v((128, 2048), BF16), v((128, 2048), BF16),
             v((2048, 128), BF16), v((2048, 128), BF16), v((1024, 256), BF16),
-            v((12, 64, 256), BF16), v((256, 256), BF16), v((2, 4, 32, 256), BF16),
+            v((12, 64, 256), BF16), v((2, 32, 256), BF16), v((256, 256), BF16), v((2, 4, 32, 256), BF16),
             v((16, 4, 32, 128), BF16), v((16, 4, 32, 128), BF16), v((16, 32, 128), BF16),
             v((16, 32, 128), BF16), v((4, 2, 16, 2048), BF16), v((4, 16, 2048), BF16),
             v((4, 16, 2048), BF16), v((4, 16, 2048), BF16),

time: 66.4 us -> 66.3 us (level)
  no operation moved by 1% of the time
where the time goes in v6:
time: 66.3 us; the launch traced here: 66.2 us
  Pallas kernels  65.5 us (99%)
    pallas_call x1, Pallas kernels, local(): pl.pallas_call(kernel, out_shape=outs, in_specs=[anywhere] * 9, out_specs...  64.6 us

profile of v6, /device:TPU:1, one launch (start us, length us, event | category | flops | bytes accessed | tf_op | source)
XLA Modules:
  0.0 66.2 jit_solution(5921243835277087754)
XLA Ops:
  0.6 64.6 %step.1 = (bf16[128,2048]{1,0:T(8,128)(2,1)S(1)}, f32[32,2048]{1,0:T(8,128)S(1)}, f32[32,128]{1,0:T(8,128)S(1)}) custom-call(bf16[128,2048]{1,0:T(8,128)(2,1)} %target.1, bf16[32,2048]{1,0:T(8,128)(2,1)} %source.1, f32[1,2048]{1,0:T(1,128)} %bitcast.2, f32[1,2048]{1,0:T(1,128)} %bitcast.3, bf16[2048,128]{1,0:T(8,128)(2,1)} %w_query.1, ...), custom_call_target="tpu_custom_call" | custom-call | tf_op jit(solution)/shard_map/step/pallas_call | solution.py:455
  65.3 0.9 %store.1 = (bf16[128,2048]{1,0:T(8,128)(2,1)}, f32[32,2048]{1,0:T(8,128)}, f32[32,128]{1,0:T(8,128)}) custom-call(bf16[128,2048]{1,0:T(8,128)(2,1)S(1)} %get-tuple-element.6.a, f32[32,2048]{1,0:T(8,128)S(1)} %get-tuple-element.7.b, f32[32,128]{1,0:T(8,128)S(1)} %get-tuple-element.8.w), custom_call_target="tpu_custom_call" | custom-call | tf_op jit(solution)/shard_map/store/pallas_call | solution.py:487

commit v7 on v6

--- a/solution.py
+++ b/solution.py
@@ -380,13 +380,13 @@
 
     z_part(0)
     z_part(1)
+    z_part(2)
+    z_part(3)
     for k, dh in ((1, 0), (3, 1)):
         via[dh].wait_recv()
         r = slice(k * 64 + dh * 32, k * 64 + dh * 32 + 32)
         far[r, :] = (far[r, :].astype(F32) + via_in[dh].astype(F32)).astype(BF16)
         far_out(k, dh)
-    z_part(2)
-    z_part(3)
     dw2[15] = dw1[15]
 
     for cp in n_send:

time: 66.3 us -> 67.6 us (1.020)
  Pallas kernels: 65.5 us -> 66.8 us
    pallas_call x1, Pallas kernels: 64.6 us -> 65.9 us  [local(): pl.pallas_call(kernel, out_shape=outs, in_specs=[anywhere] * 9, out_specs...]
where the time goes in v7:
time: 67.6 us; the launch traced here: 67.5 us
  Pallas kernels  66.8 us (99%)
    pallas_call x1, Pallas kernels, local(): pl.pallas_call(kernel, out_shape=outs, in_specs=[anywhere] * 9, out_specs...  65.9 us

profile of v7, /device:TPU:1, one launch (start us, length us, event | category | flops | bytes accessed | tf_op | source)
XLA Modules:
  0.0 67.5 jit_solution(3764788532141795188)
XLA Ops:
  0.6 65.9 %step.1 = (bf16[128,2048]{1,0:T(8,128)(2,1)S(1)}, f32[32,2048]{1,0:T(8,128)S(1)}, f32[32,128]{1,0:T(8,128)S(1)}) custom-call(bf16[128,2048]{1,0:T(8,128)(2,1)} %target.1, bf16[32,2048]{1,0:T(8,128)(2,1)} %source.1, f32[1,2048]{1,0:T(1,128)} %bitcast.2, f32[1,2048]{1,0:T(1,128)} %bitcast.3, bf16[2048,128]{1,0:T(8,128)(2,1)} %w_query.1, ...), custom_call_target="tpu_custom_call" | custom-call | tf_op jit(solution)/shard_map/step/pallas_call | solution.py:455
  66.6 0.9 %store.1 = (bf16[128,2048]{1,0:T(8,128)(2,1)}, f32[32,2048]{1,0:T(8,128)}, f32[32,128]{1,0:T(8,128)}) custom-call(bf16[128,2048]{1,0:T(8,128)(2,1)S(1)} %get-tuple-element.6.a, f32[32,2048]{1,0:T(8,128)S(1)} %get-tuple-element.7.b, f32[32,128]{1,0:T(8,128)S(1)} %get-tuple-element.8.w), custom_call_target="tpu_custom_call" | custom-call | tf_op jit(solution)/shard_map/store/pallas_call | solution.py:487
